TPU v7x, 512 devices: a whole 4x8x8 slice. The times are simulated.
512 devices in a mesh: sp: 32 (over z, x), tp: 16 (over y, core).
Axes of the slice: x: 4, y: 8, z: 8, core: 2. Of those that a mesh axis runs over, the one named last changes fastest.
Arguments:
- query_one: bfloat16 [8192, 1024], P('sp', 'tp'), may hold values from -6 to 6
- key_one: bfloat16 [8192, 1024], P('sp', 'tp'), may hold values from -6 to 6
- value_one: bfloat16 [8192, 2048], P('sp', 'tp'), may hold values from -6 to 6
- gate_one: bfloat16 [8192, 2048], P('sp', 'tp'), may hold values from -6 to 6
- decay_one: float32 [2, 8192, 1024], P(None, 'sp', 'tp')
- query_two: bfloat16 [8192, 2048], P('sp', 'tp'), may hold values from -6 to 6
- key_two: bfloat16 [8192, 2048], P('sp', 'tp'), may hold values from -6 to 6
- value_two: bfloat16 [8192, 2048], P('sp', 'tp'), may hold values from -6 to 6
- gate_two: bfloat16 [8192, 2048], P('sp', 'tp'), may hold values from -6 to 6
- decay_two: float32 [2, 8192, 2048], P(None, 'sp', 'tp')
- head_gain: float32 [128], replicated, may hold values from 0.1 to 1.9
- proj_one: bfloat16 [2048, 2048], P('tp'), may hold values from -0.09375 to 0.09375
- proj_two: bfloat16 [2048, 2048], P('tp'), may hold values from -0.09375 to 0.09375
- stream: bfloat16 [8192, 2048], P('sp'), may hold values from -6 to 6
- gain_mix: float32 [2048], replicated, may hold values from 0.1 to 1.9
- gain_moe: float32 [2048], replicated, may hold values from 0.1 to 1.9
- routes: int32 [8192, 2], P('sp'), may hold values from 0 to 31, all different within a row; in each aligned block of 256 rows (0 to 255, 256 to 511, ...) at most 24 rows name the same one
- affinity: float32 [8192, 2], P('sp'), may hold values from 0.1 to 1
- expert_gate: bfloat16 [32, 2048, 2048], P('sp', None, 'tp'), may hold values from -0.125 to 0.125
- expert_up: bfloat16 [32, 2048, 2048], P('sp', None, 'tp'), may hold values from -0.125 to 0.125
- expert_down: bfloat16 [32, 2048, 2048], P('sp', 'tp'), may hold values from -0.125 to 0.125
Outputs:
- output: bfloat16 [8192, 2048], P(('sp', 'tp'))
Inputs may be any that keep to these rules, and one draw needn't show every extreme that they name: `routes`: in the 256 rows of one index of sp no expert is named more than 24 times, a bound that some block reaches there in every draw; a row names 2 different experts.
All inputs are finite; a program needn't handle non-finite values.
Results may differ from a plain program's by a relative error of at most 0.017.
Values may be sent and summed in bfloat16 or wider, within the bound.
A program may use at most 64 MiB of HBM per device.

v0:
```python
import jax
import jax.numpy as jnp
from jax import lax
from jax.sharding import Mesh
from jax.sharding import PartitionSpec as P

DK_A = 64
DK_B = 128
BLK = 64
SP = ("sp_0", "sp_1")
SP_TP = ("sp_0", "sp_1", "tp")


normalizer_sharpness = 16.0


def neutral_like(value, identity):
    return jax.tree.map(
        lambda part, zero: jnp.zeros_like(part) + jnp.asarray(zero, part.dtype), value, identity
    )


def gathered_once(value, axis):
    leaves = jax.tree.leaves(value)
    turns = sorted(range(len(leaves)), key=lambda k: -leaves[k].size)
    width = (1, *leaves[turns[0]].shape)[-1]
    lines = [
        jnp.pad(leaves[k].reshape(-1), (0, -leaves[k].size % width)).reshape(-1, width)
        for k in turns
    ]
    both, at, found = (lax.all_gather(jnp.concatenate(lines), axis), 0, {})
    for k, line in zip(turns, lines):
        share = both[:, at : at + len(line)].reshape(len(both), -1)
        found[k] = share[:, : leaves[k].size].reshape(-1, *leaves[k].shape)
        at += len(line)
    numbers = iter(range(len(leaves)))
    return jax.tree.map(lambda _: found[next(numbers)], value)


def carried_in(value, axes, combine, identity, reverse):
    before = start = neutral_like(value, identity)
    total = value
    for axis in reversed(axes):
        peers, mine = (lax.axis_size(axis), lax.axis_index(axis))
        pieces = gathered_once(
            jax.tree.map(
                lambda part, kind: part.astype(kind),
                total,
                jax.tree.map(lambda a: jnp.bfloat16 if a.dtype == jnp.float32 else a.dtype, value),
            ),
            axis,
        )
        inside, total = (start, start)
        for k in reversed(range(peers)) if reverse else range(peers):
            passed = k > mine if reverse else k < mine
            total = combine(
                total, jax.tree.map(lambda part, own: part[k].astype(own.dtype), pieces, value)
            )
            inside = jax.tree.map(lambda new, old: jnp.where(passed, new, old), total, inside)
        before = combine(inside, before)
    return before


def split_up(value, dim, peers):
    before, after = (value.shape[:dim], value.shape[dim + 1 :])
    return jnp.moveaxis(value.reshape(*before, peers, -1, *after), dim, 0)


def summed_on_arrival(value, axis, dim):
    pieces = split_up(value, dim, lax.axis_size(axis))
    arrived = lax.all_to_all(pieces, axis, split_axis=0, concat_axis=0, tiled=True)
    return arrived.astype(jnp.float32).sum(axis=0)


def heads_first(values, heads):
    return values.reshape(values.shape[0], heads, -1).transpose(1, 0, 2)


def block_scan(query, key, value, logarithm_fading):
    heads, length, key_size = query.shape
    value_size = value.shape[-1]
    count = length // BLK

    def blocks(tensor):
        return tensor.reshape(heads, count, BLK, tensor.shape[-1])

    qb, kb, vb, gb = (blocks(query), blocks(key), blocks(value), blocks(logarithm_fading))
    cum = jnp.cumsum(gb, axis=2)
    last = cum[:, :, -1:, :]
    q_in = qb * jnp.exp(cum)
    k_in = kb * jnp.exp(-cum)
    k_st = kb * jnp.exp(last - cum)
    lower = jnp.tril(jnp.ones((BLK, BLK), dtype=bool))
    scores = jnp.where(lower, jnp.einsum("hnid,hnjd->hnij", q_in, k_in), 0.0)
    inner = jnp.einsum("hnij,hnjv->hniv", scores, vb)
    growth = jnp.einsum("hnjd,hnjv->hndv", k_st, vb)
    fading_speed = jnp.exp(last[:, :, 0, :])

    def step(state, inputs):
        factor, added = inputs
        return (factor[..., None] * state + added, state)

    final, starts = lax.scan(
        step,
        jnp.zeros((heads, key_size, value_size), jnp.float32),
        (fading_speed.transpose(1, 0, 2), growth.transpose(1, 0, 2, 3)),
    )
    carried = jnp.einsum("hnid,hndv->hniv", q_in, starts.transpose(1, 0, 2, 3))
    return ((inner + carried).reshape(heads, length, value_size), final)


def group_local(query, key, value, fading_speed, key_size):
    heads = query.shape[1] // key_size
    qh = heads_first(query.astype(jnp.float32), heads) * key_size ** (-0.5)
    kh = heads_first(key.astype(jnp.float32), heads)
    vh = heads_first(value.astype(jnp.float32), heads)
    logarithm_fading = jax.nn.log_sigmoid(fading_speed) / normalizer_sharpness
    ahead = heads_first(logarithm_fading[0], heads)
    behind = heads_first(logarithm_fading[1], heads)[:, ::-1]
    flipped_q = qh[:, ::-1]
    forward, state_ahead = block_scan(qh, kh, vh, ahead)
    backward, state_behind = block_scan(flipped_q, kh[:, ::-1], vh[:, ::-1], behind)
    cum_ahead = jnp.cumsum(ahead, axis=1)
    cum_behind = jnp.cumsum(behind, axis=1)
    reader_ahead = qh * jnp.exp(cum_ahead)
    reader_behind = flipped_q * jnp.exp(cum_behind)
    return (
        forward,
        backward,
        reader_ahead,
        reader_behind,
        cum_ahead[:, -1, :],
        cum_behind[:, -1, :],
        state_ahead,
        state_behind,
    )


def chain(earlier, later):
    return (
        earlier[0] + later[0],
        jnp.exp(later[0])[..., None] * earlier[1] + later[1],
        earlier[2] + later[2],
        jnp.exp(later[2])[..., None] * earlier[3] + later[3],
    )


def readout(reader, state):
    return jnp.einsum("htd,hdv->htv", reader, state)


def finish(mixed, gate, head_gain):
    normed = mixed * lax.rsqrt(jnp.mean(mixed * mixed, axis=-1, keepdims=True) + 1e-06) * head_gain
    flat = normed.transpose(1, 0, 2).reshape(mixed.shape[1], -1)
    return (flat * jax.nn.silu(gate.astype(jnp.float32))).astype(jnp.bfloat16)


def layer_norm(values, gain):
    mean = jnp.mean(values, axis=-1, keepdims=True)
    spread = jnp.mean(jnp.square(values - mean), axis=-1, keepdims=True)
    return (values - mean) * lax.rsqrt(spread + 1e-05) * gain


def body(
    query_one,
    key_one,
    value_one,
    gate_one,
    decay_one,
    query_two,
    key_two,
    value_two,
    gate_two,
    decay_two,
    head_gain,
    proj_one,
    proj_two,
    stream,
    gain_mix,
    gain_moe,
    routes,
    affinity,
    expert_gate,
    expert_up,
    expert_down,
):
    rows = query_one.shape[0]
    tp_count = lax.axis_size("tp")
    tp_rank = lax.axis_index("tp")
    sp_count = lax.axis_size(SP)
    own_rows = rows // tp_count
    first = group_local(query_one, key_one, value_one, decay_one, DK_A)
    second = group_local(query_two, key_two, value_two, decay_two, DK_B)
    ahead_in = (first[4], first[6], second[4], second[6])
    behind_in = (first[5], first[7], second[5], second[7])
    empty = tuple((jnp.zeros_like(item) for item in ahead_in))
    from_left = carried_in(ahead_in, SP, chain, empty, False)
    from_right = carried_in(behind_in, SP, chain, empty, True)
    mixed_one = (
        first[0]
        + readout(first[2], from_left[1])
        + (first[1] + readout(first[3], from_right[1]))[:, ::-1]
    )
    mixed_two = (
        second[0]
        + readout(second[2], from_left[3])
        + (second[1] + readout(second[3], from_right[3]))[:, ::-1]
    )
    heads_one = finish(mixed_one, gate_one, head_gain)
    heads_two = finish(mixed_two, gate_two, head_gain)
    part = jnp.dot(heads_one, proj_one, preferred_element_type=jnp.float32)
    attn = summed_on_arrival(
        (part + jnp.dot(heads_two, proj_two, preferred_element_type=jnp.float32)).astype(
            jnp.bfloat16
        ),
        "tp",
        0,
    ).astype(jnp.bfloat16)
    stream_own = lax.dynamic_slice_in_dim(stream, tp_rank * own_rows, own_rows, 0)
    settled_own = layer_norm(stream_own.astype(jnp.float32) + attn.astype(jnp.float32), gain_mix)
    moe_in = lax.all_gather(settled_own.astype(jnp.bfloat16), "tp", axis=0, tiled=True)
    top_count = routes.shape[1]
    local_experts = expert_gate.shape[0]
    expert_total = local_experts * sp_count
    capacity = 3 * rows * top_count // (2 * expert_total)
    width = moe_in.shape[1]
    slice_width = width // tp_count
    flat_expert = routes.reshape(-1)
    weights = affinity / jnp.sum(affinity, axis=-1, keepdims=True)
    flat_weights = weights.reshape(-1)
    onehot = (flat_expert[:, None] == jnp.arange(expert_total, dtype=jnp.int32)[None, :]).astype(
        jnp.int32
    )
    rank = jnp.sum(jnp.cumsum(onehot, axis=0) * onehot, axis=1) - 1
    target = flat_expert * capacity + rank
    token = jnp.arange(rows * top_count, dtype=jnp.int32) // top_count
    columns = lax.dynamic_slice_in_dim(moe_in, tp_rank * slice_width, slice_width, 1)
    outgoing = (
        jnp.zeros((expert_total * capacity, slice_width), jnp.bfloat16)
        .at[target]
        .set(columns[token])
    )
    outgoing = outgoing.reshape(sp_count, local_experts, capacity, slice_width)
    arrived = lax.all_to_all(outgoing, SP, split_axis=0, concat_axis=0, tiled=True)
    complete = lax.all_gather(arrived, "tp", axis=3, tiled=True)
    gate = jnp.einsum("secd,edf->secf", complete, expert_gate, preferred_element_type=jnp.float32)
    upward = jnp.einsum("secd,edf->secf", complete, expert_up, preferred_element_type=jnp.float32)
    act = (jax.nn.silu(gate) * upward).astype(jnp.bfloat16)
    partial_value = jnp.einsum(
        "secf,efd->secd", act, expert_down, preferred_element_type=jnp.float32
    ).astype(jnp.bfloat16)
    summed = summed_on_arrival(
        partial_value.astype(jnp.float32).astype(jnp.bfloat16), "tp", 3
    ).astype(jnp.bfloat16)
    returned = lax.all_to_all(summed, SP, split_axis=0, concat_axis=0, tiled=True)
    pieces = returned.reshape(expert_total * capacity, slice_width)[target]
    weighted = pieces.astype(jnp.float32) * flat_weights[:, None]
    term = jnp.sum(weighted.reshape(rows, top_count, slice_width), axis=1)
    mixture = lax.all_to_all(
        term.astype(jnp.bfloat16), "tp", split_axis=0, concat_axis=1, tiled=True
    ).astype(term.dtype)
    return layer_norm(settled_own + mixture, gain_moe).astype(jnp.bfloat16)


def solution(mesh):
    finer = Mesh(mesh.devices.reshape(8, 4, mesh.shape["tp"]), ("sp_0", "sp_1", "tp"))
    return jax.shard_map(
        body,
        mesh=finer,
        in_specs=(
            P(SP, "tp"),
            P(SP, "tp"),
            P(SP, "tp"),
            P(SP, "tp"),
            P(None, SP, "tp"),
            P(SP, "tp"),
            P(SP, "tp"),
            P(SP, "tp"),
            P(SP, "tp"),
            P(None, SP, "tp"),
            P(),
            P("tp", None),
            P("tp", None),
            P(SP, None),
            P(),
            P(),
            P(SP, None),
            P(SP, None),
            P(SP, None, "tp"),
            P(SP, None, "tp"),
            P(SP, "tp", None),
        ),
        out_specs=P(SP_TP, None),
        check_vma=False,
    )
```

profile of v0, /device:TPU:1, one launch (start us, length us, event | category | flops | bytes accessed | tf_op | source)
XLA Modules:
  0.0 402.3 jit_solution(4113022673467742287)
XLA Ops:
  6.6 1.1 fusion.56
  8.8 1.1 fusion.42
  16.2 10.4 %all-gather.4 = bf16[4,194,128]{2,1,0:T(8,128)(2,1)S(1)} all-gather(bf16[1,194,128]{2,1,0:T(8,128)(2,1)S(1)} %maximum_bitcast_fusion), channel_id=2, replica_groups=mesh['sp_0'=8,'sp_1'=4,'tp'=16] {'sp_1'}, dimensions={0}, use_global_device_ids=true | all-gather | bytes 248320 | tf_op jit(solution)/shard_map/all_gather | solution.py:31
  28.1 25.9 %all-gather.5 = bf16[8,194,128]{2,1,0:T(8,128)(2,1)S(1)} all-gather(bf16[1,194,128]{2,1,0:T(8,128)(2,1)S(1)} %maximum_bitcast_fusion.1), channel_id=3, replica_groups=mesh['sp_0'=8,'sp_1'=4,'tp'=16] {'sp_0'}, dimensions={0}, use_global_device_ids=true | all-gather | bytes 446976 | tf_op jit(solution)/shard_map/all_gather | solution.py:31
  58.1 9.6 %all-gather.6 = bf16[4,194,128]{2,1,0:T(8,128)(2,1)S(1)} all-gather(bf16[1,194,128]{2,1,0:T(8,128)(2,1)S(1)} %maximum_bitcast_fusion.2), channel_id=4, replica_groups=mesh['sp_0'=8,'sp_1'=4,'tp'=16] {'sp_1'}, dimensions={0}, use_global_device_ids=true | all-gather | bytes 248320 | tf_op jit(solution)/shard_map/all_gather | solution.py:31
  69.5 19.1 %all-gather.7 = bf16[8,194,128]{2,1,0:T(8,128)(2,1)S(1)} all-gather(bf16[1,194,128]{2,1,0:T(8,128)(2,1)S(1)} %maximum_bitcast_fusion.3), channel_id=5, replica_groups=mesh['sp_0'=8,'sp_1'=4,'tp'=16] {'sp_0'}, dimensions={0}, use_global_device_ids=true | all-gather | bytes 446976 | tf_op jit(solution)/shard_map/all_gather | solution.py:31
  89.4 1.5 reverse.26
  93.1 1.5 convolution_add_fusion.3
  95.6 1.4 multiply_reduce_fusion.2
  99.9 1.4 convolution_add_fusion.7
  102.2 1.4 multiply_reduce_fusion.3
  106.1 1.5 fusion.8
  107.6 25.2 %all-to-all-start = ((bf16[16,16,2048]{2,1,0:T(8,128)(2,1)}), bf16[16,16,2048]{2,1,0:T(8,128)(2,1)S(1)}, u32[]{:S(2)}, u32[]{:S(2)}) async-start(bf16[16,16,2048]{2,1,0:T(8,128)(2,1)} %bitcast.161), calls=%async_computation | async-start | bytes 2097152 | tf_op jit(solution)/shard_map/all_to_all | solution.py:71
  132.8 27.9 %all-to-all-done = bf16[16,16,2048]{2,1,0:T(8,128)(2,1)S(1)} async-done(((bf16[16,16,2048]{2,1,0:T(8,128)(2,1)}), bf16[16,16,2048]{2,1,0:T(8,128)(2,1)S(1)}, u32[]{:S(2)}, u32[]{:S(2)}) %all-to-all-start) | async-done | bytes 1048608 | tf_op jit(solution)/shard_map/all_to_all | solution.py:71
  160.9 1.0 fusion.107
  161.9 1.0 multiply_reduce_fusion.1
  163.0 1.6 fusion.110
  165.3 1.2 reduce-window.46
  167.2 32.0 %all-gather.11.cloned.1.call-done = bf16[256,2048]{1,0:T(8,128)(2,1)} async-done(((bf16[16,2048]{1,0:T(8,128)(2,1)}), bf16[256,2048]{1,0:T(8,128)(2,1)}) %all-gather.11.cloned.1.call-update) | async-done | bytes 1048592 | tf_op jit(solution)/shard_map/all_gather | solution.py:221
  200.1 3.0 scatter_custom_fusion
  203.1 20.4 %all_to_all.30 = bf16[32,1,24,128]{3,2,1,0:T(8,128)(2,1)} all-to-all(bf16[32,1,24,128]{3,2,1,0:T(8,128)(2,1)S(1)} %bitcast.615), channel_id=1, replica_groups=mesh['sp_0'=8,'sp_1'=4,'tp'=16] {'sp_0','sp_1'}, dimensions={0} | all-to-all | bytes 393216 | tf_op jit(solution)/shard_map/all_to_all | solution.py:244
  223.5 42.4 %all-gather.13.cloned.1.call-done = bf16[32,1,24,2048]{3,2,0,1:T(8,128)(2,1)} async-done(((bf16[32,1,24,128]{3,2,0,1:T(8,128)(2,1)}), bf16[32,1,24,2048]{3,2,0,1:T(8,128)(2,1)}) %all-gather.13.cloned.1.call-update) | async-done | bytes 3145744 | tf_op jit(solution)/shard_map/all_gather | solution.py:245
  265.9 2.9 fusion.10
  268.8 6.9 %fusion.9 = bf16[1,32,3,16,8,128]{5,4,3,2,1,0:T(8,128)(2,1)} fusion(bf16[32,1,24,2048]{3,2,0,1:T(8,128)(2,1)} %all-gather.13.cloned.1.call-done, bf16[1,128,2048]{2,1,0:T(8,128)(2,1)S(1)} %copy-done, bf16[1,2048,128]{2,1,0:T(8,128)(2,1)S(1)} %copy-done.6, f32[32,1,24,128]{3,2,0,1:T(8,128)S(1)} %fusion.10), kind=kOutput, calls=%fused_computation.27 | convolution fusion | flops 807469056 | bytes 7733248 | tf_op jit(solution)/shard_map/secf,efd->secd/dot_general | solution.py:249
  275.8 2.7 copy.353
  278.5 77.5 %all_to_all.31 = bf16[16,32,1,24,128]{4,3,1,2,0:T(8,128)(2,1)} all-to-all(bf16[16,32,1,24,128]{4,3,1,2,0:T(8,128)(2,1)S(1)} %bitcast.592), channel_id=1, replica_groups=mesh['sp_0'=8,'sp_1'=4,'tp'=16] {'tp'}, dimensions={0} | all-to-all | bytes 6291456 | tf_op jit(solution)/shard_map/all_to_all | solution.py:71
  356.0 3.1 reduce_sum.113
  359.1 9.9 %all-to-all-start.3 = ((bf16[32,1,24,128]{3,2,1,0:T(8,128)(2,1)}), bf16[32,1,24,128]{3,2,1,0:T(8,128)(2,1)S(1)}, u32[]{:S(2)}, u32[]{:S(2)}) async-start(bf16[32,1,24,128]{3,2,1,0:T(8,128)(2,1)} %bitcast.188), calls=%async_computation.3 | async-start | bytes 393216 | tf_op jit(solution)/shard_map/all_to_all | solution.py:255
  369.2 11.4 %all-to-all-done.3 = bf16[32,1,24,128]{3,2,1,0:T(8,128)(2,1)S(1)} async-done(((bf16[32,1,24,128]{3,2,1,0:T(8,128)(2,1)}), bf16[32,1,24,128]{3,2,1,0:T(8,128)(2,1)S(1)}, u32[]{:S(2)}, u32[]{:S(2)}) %all-to-all-start.3) | async-done | bytes 196640 | tf_op jit(solution)/shard_map/all_to_all | solution.py:255
  380.6 1.3 gather_fusion
  382.4 11.1 %all_to_all.32 = bf16[16,16,128]{2,1,0:T(8,128)(2,1)S(1)} all-to-all(bf16[16,16,128]{2,1,0:T(8,128)(2,1)S(1)} %bitcast.635), channel_id=1, replica_groups=mesh['sp_0'=8,'sp_1'=4,'tp'=16] {'tp'}, dimensions={0} | all-to-all | bytes 131072 | tf_op jit(solution)/shard_map/all_to_all | solution.py:259
  393.4 1.0 fusion.521
  (332 shorter events, 29.5 us)
Async XLA Ops:
  6.5 262.3 %copy-start = (bf16[1,128,2048]{2,1,0:T(8,128)(2,1)S(1)}, bf16[1,128,2048]{2,1,0:T(8,128)(2,1)}, u32[]{:S(2)}) copy-start(bf16[1,128,2048]{2,1,0:T(8,128)(2,1)} %param.49) | copy-start | bytes 1572868
  8.8 48.3 %copy-start.15 = (f32[1,64,2,128]{3,2,0,1:T(2,128)}, f32[1,64,2,128]{3,2,0,1:T(2,128)S(1)}, u32[]{:S(2)}) copy-start(f32[1,64,2,128]{3,2,0,1:T(2,128)S(1)} %copy.288) | copy-start | bytes 196612
  27.8 26.2 %copy-start.24 = (f32[64]{0:T(128)}, f32[64]{0:T(128)S(1)}, u32[]{:S(2)}) copy-start(f32[64]{0:T(128)S(1)} %get-tuple-element.448) | copy-start | bytes 772
  57.1 32.3 %copy-start.17 = (f32[1,64,256]{2,1,0:T(8,128)}, f32[1,64,256]{2,1,0:T(8,128)S(1)}, u32[]{:S(2)}) copy-start(f32[1,64,256]{2,1,0:T(8,128)S(1)} %reshape.2436) | copy-start | bytes 196612
  68.8 26.6 %copy-start.26 = (f32[64]{0:T(128)}, f32[64]{0:T(128)S(1)}, u32[]{:S(2)}) copy-start(f32[64]{0:T(128)S(1)} %get-tuple-element.451) | copy-start | bytes 772
  69.5 26.0 %copy-start.19 = (f32[1,128,256]{1,2,0:T(8,128)S(1)}, f32[1,128,256]{1,2,0:T(8,128)}, u32[]{:S(2)}) copy-start(f32[1,128,256]{1,2,0:T(8,128)} %get-tuple-element.413) | copy-start | bytes 393220
  69.5 26.0 %copy-start.33 = (f32[128]{0:T(128)S(1)}, f32[128]{0:T(128)}, u32[]{:S(2)}) copy-start(f32[128]{0:T(128)} %copy-done.32) | copy-start | bytes 1540
  69.5 26.0 %copy-start.35 = (f32[128]{0:T(128)S(1)}, f32[128]{0:T(128)}, u32[]{:S(2)}) copy-start(f32[128]{0:T(128)} %copy-done.34) | copy-start | bytes 1540
  69.5 26.0 %copy-start.37 = (f32[128]{0:T(128)S(1)}, f32[128]{0:T(128)}, u32[]{:S(2)}) copy-start(f32[128]{0:T(128)} %copy-done.36) | copy-start | bytes 1540
  69.5 26.0 %copy-start.39 = (f32[128]{0:T(128)S(1)}, f32[128]{0:T(128)}, u32[]{:S(2)}) copy-start(f32[128]{0:T(128)} %copy-done.38) | copy-start | bytes 1540
  88.6 6.9 %copy-start.42 = (f32[128]{0:T(128)S(1)}, f32[128]{0:T(128)}, u32[]{:S(2)}) copy-start(f32[128]{0:T(128)} %get-tuple-element.379) | copy-start | bytes 1540
  88.6 6.9 %copy-start.43 = (f32[128]{0:T(128)S(1)}, f32[128]{0:T(128)}, u32[]{:S(2)}) copy-start(f32[128]{0:T(128)} %get-tuple-element.387) | copy-start | bytes 1540
  88.6 6.9 %copy-start.44 = (f32[128]{0:T(128)S(1)}, f32[128]{0:T(128)}, u32[]{:S(2)}) copy-start(f32[128]{0:T(128)} %get-tuple-element.388) | copy-start | bytes 1540
  88.6 6.9 %copy-start.45 = (f32[128]{0:T(128)S(1)}, f32[128]{0:T(128)}, u32[]{:S(2)}) copy-start(f32[128]{0:T(128)} %get-tuple-element.389) | copy-start | bytes 1540
  88.7 6.9 %copy-start.46 = (f32[128]{0:T(128)S(1)}, f32[128]{0:T(128)}, u32[]{:S(2)}) copy-start(f32[128]{0:T(128)} %get-tuple-element.390) | copy-start | bytes 1540
  88.7 6.9 %copy-start.47 = (f32[128]{0:T(128)S(1)}, f32[128]{0:T(128)}, u32[]{:S(2)}) copy-start(f32[128]{0:T(128)} %get-tuple-element.391) | copy-start | bytes 1540
  88.7 6.9 %copy-start.48 = (f32[128]{0:T(128)S(1)}, f32[128]{0:T(128)}, u32[]{:S(2)}) copy-start(f32[128]{0:T(128)} %get-tuple-element.392) | copy-start | bytes 1540
  88.7 6.9 %copy-start.49 = (f32[128]{0:T(128)S(1)}, f32[128]{0:T(128)}, u32[]{:S(2)}) copy-start(f32[128]{0:T(128)} %get-tuple-element.393) | copy-start | bytes 1540
  88.7 6.9 %copy-start.50 = (f32[128]{0:T(128)S(1)}, f32[128]{0:T(128)}, u32[]{:S(2)}) copy-start(f32[128]{0:T(128)} %get-tuple-element.394) | copy-start | bytes 1540
  93.1 6.8 %copy-start.16 = (f32[1,64,2,128]{3,2,0,1:T(2,128)S(1)}, f32[1,64,2,128]{3,2,0,1:T(2,128)}, u32[]{:S(2)}) copy-start(f32[1,64,2,128]{3,2,0,1:T(2,128)} %copy-done.15) | copy-start | bytes 196612
  97.1 8.4 %copy-start.4 = (bf16[128,2048]{1,0:T(8,128)(2,1)S(1)}, bf16[128,2048]{1,0:T(8,128)(2,1)}, u32[]{:S(2)}) copy-start(bf16[128,2048]{1,0:T(8,128)(2,1)} %param.40) | copy-start | bytes 1572868
  97.1 8.4 %copy-start.41 = (f32[128]{0:T(128)S(1)}, f32[128]{0:T(128)}, u32[]{:S(2)}) copy-start(f32[128]{0:T(128)} %param.39) | copy-start | bytes 1540
  106.1 56.9 %copy-start.20 = (f32[2048]{0:T(1024)S(1)}, f32[2048]{0:T(1024)}, u32[]{:S(2)}) copy-start(f32[2048]{0:T(1024)} %param.43) | copy-start | bytes 24580
  106.1 58.8 %copy-start.21 = (s32[256,2]{0,1:T(2,128)S(1)}, s32[256,2]{0,1:T(2,128)}, u32[]{:S(2)}) copy-start(s32[256,2]{0,1:T(2,128)} %param.45) | copy-start | bytes 6148
  107.6 158.3 %copy-start.5 = (bf16[1,2048,128]{2,1,0:T(8,128)(2,1)S(1)}, bf16[1,2048,128]{2,1,0:T(8,128)(2,1)}, u32[]{:S(2)}) copy-start(bf16[1,2048,128]{2,1,0:T(8,128)(2,1)} %param.47) | copy-start | bytes 1572868
  107.6 53.2 %all-to-all-start = ((bf16[16,16,2048]{2,1,0:T(8,128)(2,1)}), bf16[16,16,2048]{2,1,0:T(8,128)(2,1)S(1)}, u32[]{:S(2)}, u32[]{:S(2)}) async-start(bf16[16,16,2048]{2,1,0:T(8,128)(2,1)} %bitcast.161), calls=%async_computation | async-start | bytes 2097152 | tf_op jit(solution)/shard_map/all_to_all | solution.py:71
  132.8 66.4 %all-gather.11.cloned.1.call-start = ((), (), s32[]{:S(2)}) async-start(), calls=%async_computation.5 | async-start | bytes 1114112 | tf_op jit(solution)/shard_map/all_gather | solution.py:221
  163.0 105.9 %copy-start.6 = (bf16[1,2048,128]{2,1,0:T(8,128)(2,1)S(1)}, bf16[1,2048,128]{2,1,0:T(8,128)(2,1)}, u32[]{:S(2)}) copy-start(bf16[1,2048,128]{2,1,0:T(8,128)(2,1)} %param.48) | copy-start | bytes 1572868
  164.6 101.3 %all-gather.13.cloned.1.call-start = ((), (), s32[]{:S(2)}) async-start(), calls=%async_computation.6 | async-start | bytes 3342336 | tf_op jit(solution)/shard_map/all_gather | solution.py:245
  356.0 12.9 %copy-start.23 = (f32[256,2]{0,1:T(2,128)S(1)}, f32[256,2]{0,1:T(2,128)}, u32[]{:S(2)}) copy-start(f32[256,2]{0,1:T(2,128)} %param.46) | copy-start | bytes 6148
  356.0 38.7 %copy-start.22 = (f32[2048]{0:T(1024)S(1)}, f32[2048]{0:T(1024)}, u32[]{:S(2)}) copy-start(f32[2048]{0:T(1024)} %param.44) | copy-start | bytes 24580
  359.1 21.5 %all-to-all-start.3 = ((bf16[32,1,24,128]{3,2,1,0:T(8,128)(2,1)}), bf16[32,1,24,128]{3,2,1,0:T(8,128)(2,1)S(1)}, u32[]{:S(2)}, u32[]{:S(2)}) async-start(bf16[32,1,24,128]{3,2,1,0:T(8,128)(2,1)} %bitcast.188), calls=%async_computation.3 | async-start | bytes 393216 | tf_op jit(solution)/shard_map/all_to_all | solution.py:255
  (30 other events, 101.7 us)
Sparse Core Ops, SparseCore 0:
  164.7 34.4 all-gather.10
  223.7 42.2 all-gather.12
where the time goes:
time: 403 us; the launch traced here: 402 us
  blocking collectives  174 us (43%)
  waiting for transfers between devices  114 us (28%)
  starting transfers between devices  35.3 us (9%)
  other arithmetic  25.8 us (6%)
  matrix products  20.4 us (5%)
  local copies, waits for them, and re-layouts  17.7 us (4%)
  between operations  14.9 us (4%)
    all_to_all x1, blocking collectives, summed_on_arrival(): lax.all_to_all(pieces, axis, split_axis=0, concat_axis=0, tiled=True)  77.5 us
    all_gather x4, blocking collectives, gathered_once(): both, at, found = (lax.all_gather(jnp.concatenate(lines), axis), 0, {})  65 us
    all_gather x1, waiting for transfers between devices, body(): complete = lax.all_gather(arrived, 'tp', axis=3, tiled=True)  42.4 us
    all_gather x1, waiting for transfers between devices, body(): lax.all_gather(settled_own.astype(jnp.bfloat16), 'tp', axis=0, tiled=True)  32 us
    all_to_all x1, waiting for transfers between devices, summed_on_arrival(): lax.all_to_all(pieces, axis, split_axis=0, concat_axis=0, tiled=True)  27.9 us
    all_to_all x1, starting transfers between devices, summed_on_arrival(): lax.all_to_all(pieces, axis, split_axis=0, concat_axis=0, tiled=True)  25.2 us
    all_to_all x1, blocking collectives, body(): lax.all_to_all(outgoing, SP, split_axis=0, concat_axis=0, tiled=True)  20.4 us
    all_to_all x1, waiting for transfers between devices, body(): lax.all_to_all(summed, SP, split_axis=0, concat_axis=0, tiled=True)  11.4 us
  transfers between devices with their start and end apart: 4, of which 4 were waited for; matrix products, arithmetic and copies ran while one was open for 1% of the time, Pallas kernels for 0%

commit v1 on v0

v1 whole, which is shorter than its diff:
```python
import functools

import jax
import jax.numpy as jnp
from jax import lax
from jax.experimental import pallas as pl
from jax.experimental.pallas import tpu as pltpu
from jax.sharding import PartitionSpec as P

MESH = pl.DeviceIdType.MESH
F32 = jnp.float32
BF16 = jnp.bfloat16
BLK = 64
LANES = 128
ANY = pl.ANY


def mm(a, b):
    return jnp.dot(a, b, preferred_element_type=F32)


def mm_t(a, b):
    return lax.dot_general(a, b, (((1,), (1,)), ((), ())), preferred_element_type=F32)


def tmm(a, b):
    return lax.dot_general(a, b, (((0,), (0,)), ((), ())), preferred_element_type=F32)


def iota(shape, dim):
    return lax.broadcasted_iota(jnp.int32, shape, dim)


def layer_norm(values, gain):
    mean = jnp.mean(values, axis=-1, keepdims=True)
    spread = jnp.mean(jnp.square(values - mean), axis=-1, keepdims=True)
    return (values - mean) * lax.rsqrt(spread + 1e-05) * gain


def kernel(
    cfg,
    q1h, k1h, v1h, g1h, d1h, q2h, k2h, v2h, g2h, d2h, hgh, p1h, p2h, sth, gmh, goh, rth, afh, egh, euh, edh,
    out,
    q1, k1, v1, g1, d1, q2, k2, v2, g2, d2, hg, own_proj, other_proj, stream, gm, go, rt, af, wgu, own_down, other_down,
    sbuf, sarr, fsum, sret, sback,
    qin, kin, grow, mixed, heads, heads_in, part,
    pbuf, parr, settled, msend, cols, dsend, darr, rows, acc, act, act_in, rbuf, rarr, rsend, rback,
    pick_hi, pick_lo, term, mix,
    load_sem, s_send, s_recv, sib_send, sib_recv, p_send, p_recv, t_send, t_recv,
    g_send, g_recv, f_send, f_recv, r_send, r_recv,
):
    nsp, ntp, toks, cap = cfg
    ny = ntp // 2
    half_way = ny // 2
    sp = lax.axis_index("sp")
    tp = lax.axis_index("tp")
    y = lax.div(tp, 2)
    c = lax.rem(tp, 2)
    sib = (sp, tp + 1 - 2 * c)
    blocks = toks // BLK
    own_rows = toks // ntp
    width = ntp * LANES
    per = LANES // nsp
    mrow = sbuf.shape[1]
    nrow = nsp * cap
    hrow = nrow // 2

    barrier = pltpu.get_barrier_semaphore()

    def greet_sp(k, carry):
        pl.semaphore_signal(barrier, inc=1, device_id=(lax.rem(sp + k, nsp), tp), device_id_type=MESH)
        return carry

    def greet_tp(k, carry):
        pl.semaphore_signal(barrier, inc=1, device_id=(sp, lax.rem(tp + k, ntp)), device_id_type=MESH)
        return carry

    lax.fori_loop(1, nsp, greet_sp, 0)
    lax.fori_loop(1, ntp, greet_tp, 0)

    loads = []

    def load(src, dst):
        copy = pltpu.make_async_copy(src, dst, load_sem.at[len(loads)])
        copy.start()
        loads.append(copy)
        return copy

    first = [load(a, b) for a, b in ((d1h, d1), (d2h, d2), (k1h, k1), (v1h, v1), (k2h, k2), (v2h, v2), (q1h, q1), (q2h, q2))]
    second = [
        load(a, b)
        for a, b in (
            (g1h, g1), (g2h, g2), (hgh, hg), (p1h, own_proj.at[0:LANES]), (p2h, own_proj.at[LANES:2 * LANES]),
            (sth.at[pl.ds(pl.multiple_of(tp * own_rows, own_rows), own_rows)], stream), (gmh, gm), (goh, go),
            (rth, rt), (afh, af),
            (egh.at[0], wgu.at[:, 0:LANES]), (euh.at[0], wgu.at[:, LANES:2 * LANES]), (edh.at[0], own_down),
        )
    ]

    r = iota((toks, toks), 0)
    s = iota((toks, toks), 1)
    tri = jnp.where((r // BLK == s // BLK) & (s <= r), 1.0, 0.0).astype(BF16)
    low = iota((1, LANES), 1) < LANES // 2
    m = iota((nsp * mrow, LANES), 0)
    o, i = m // mrow, m % mrow
    wanted = jnp.where(i < 3 * per, (i // per) * LANES + o * per + i % per, 3 * LANES + i - 3 * per)
    wanted = jnp.where(i < 3 * per + 3, wanted, -1)
    lane = iota((nsp * mrow, LANES), 1)
    pack = [jnp.where(wanted == lane + g * LANES, 1.0, 0.0).astype(BF16) for g in range(3)]
    lane16 = iota((nsp * mrow, 16), 1)
    pack.append(jnp.where(wanted[:, 0:16] == lane16 + 3 * LANES, 1.0, 0.0).astype(BF16))

    for copy in first:
        copy.wait()

    def two(a):
        return jnp.concatenate([a, a], axis=1)

    fading = (jnp.concatenate([d1[0], d1[1]], axis=1), d2[0], d2[1])
    keys = (two(k1[...].astype(F32)), k2[...].astype(F32), k2[...].astype(F32))
    queries = (two(q1[...].astype(F32)) * 64 ** (-0.5), q2[...].astype(F32) * 128 ** (-0.5), q2[...].astype(F32) * 128 ** (-0.5))
    values = (v1[...], v2[...], v2[...])
    totals = []
    for g in range(3):
        x = fading[g]
        logs = (jnp.minimum(x, 0.0) - jnp.log1p(jnp.exp(-jnp.abs(x)))) * (1.0 / 16.0)
        hi = logs.astype(BF16)
        rest = logs - hi.astype(F32)
        mid = rest.astype(BF16)
        lo = (rest - mid.astype(F32)).astype(BF16)
        cum = mm(tri, hi) + mm(tri, mid) + mm(tri, lo)
        rows_of = []
        for b in range(blocks):
            at = slice(b * BLK, (b + 1) * BLK)
            ahead = cum[at]
            tot = ahead[BLK - 1:BLK]
            behind = tot - ahead + logs[at]
            run = ahead if g == 1 else behind if g == 2 else jnp.where(low, ahead, behind)
            qin[g, at] = (queries[g][at] * jnp.exp(run)).astype(BF16)
            kin[g, at] = (keys[g][at] * jnp.exp(-run)).astype(BF16)
            kst = (keys[g][at] * jnp.exp(tot - run)).astype(BF16)
            grow[g, b] = tmm(values[g][at], kst)
            rows_of.append(tot)
        totals.append(rows_of)

    fades = [[jnp.exp(t) for t in row] for row in totals]

    def chained(g, order, start):
        state = start
        seen = {}
        for b in order:
            seen[b] = state
            state = fades[g][b] * state + grow[g, b]
        return seen, state

    up, down = list(range(blocks)), list(range(blocks - 1, -1, -1))
    zero = jnp.zeros((LANES, LANES), F32)
    ends = [
        jnp.where(low, chained(0, up, zero)[1], chained(0, down, zero)[1]),
        chained(1, up, zero)[1],
        chained(2, down, zero)[1],
    ]
    sums = [sum(row[1:], row[0]) for row in totals]
    r16 = iota((16, LANES), 0)
    tail = jnp.where(r16 == 0, sums[0], jnp.where(r16 == 1, sums[1], jnp.where(r16 == 2, sums[2], 0.0)))
    packed = mm(pack[3], tail.astype(BF16))
    for g in range(3):
        packed = packed + mm(pack[g], ends[g].astype(BF16))
    sbuf[...] = packed.astype(BF16).reshape(nsp, mrow, LANES)

    pl.semaphore_wait(barrier, nsp - 1 + ntp - 1)

    def over_sp(base, src, dst, size):
        def copy_to(k):
            to = lax.rem(sp + k, nsp)
            return pltpu.make_async_remote_copy(
                src.at[pl.ds(to * size, size)], dst.at[pl.ds(sp * size, size)],
                s_send.at[base * nsp + k], s_recv.at[base * nsp + k], device_id=(to, tp), device_id_type=MESH,
            )

        def go_out(k, carry):
            copy_to(k).start()
            return carry

        def come_in(k, carry):
            copy_to(k).wait_recv()
            return carry

        def left(k, carry):
            copy_to(k).wait_send()
            return carry

        return go_out, come_in, left

    pending = []

    def send_sp(base, src, dst, size):
        go_out, come_in, left = over_sp(base, src, dst, size)
        lax.fori_loop(1, nsp, go_out, 0)
        dst[pl.ds(sp * size, size)] = src[pl.ds(sp * size, size)]
        pending.append(lambda: lax.fori_loop(1, nsp, left, 0))
        return lambda: lax.fori_loop(1, nsp, come_in, 0)

    remote = []

    def push(src, dst, ssem, rsem, device):
        copy = pltpu.make_async_remote_copy(src, dst, ssem, rsem, device_id=device, device_id_type=MESH)
        copy.start()
        remote.append(copy)
        return copy

    arrive = send_sp(0, sbuf, sarr, 1)
    lend = [
        push(p1h, other_proj.at[0:LANES], sib_send.at[0], sib_recv.at[0], sib),
        push(p2h, other_proj.at[LANES:2 * LANES], sib_send.at[1], sib_recv.at[1], sib),
        push(edh.at[0], other_down, sib_send.at[2], sib_recv.at[2], sib),
    ]

    rr, cc = iota((BLK, BLK), 0), iota((BLK, BLK), 1)
    lower, upper = cc <= rr, cc >= rr
    for b in range(blocks):
        at = slice(b * BLK, (b + 1) * BLK)
        q, k = qin[0, at], kin[0, at]
        nil = jnp.zeros_like(q)
        score = jnp.where(lower, mm_t(jnp.where(low, q, nil), k), 0.0) + jnp.where(upper, mm_t(jnp.where(low, nil, q), k), 0.0)
        mixed[0, at] = mm(score.astype(BF16), values[0][at])
        score = jnp.where(lower, mm_t(qin[1, at], kin[1, at]), 0.0) + jnp.where(upper, mm_t(qin[2, at], kin[2, at]), 0.0)
        mixed[1, at] = mm(score.astype(BF16), values[1][at])

    arrive()
    row = iota((mrow, LANES), 0)
    in_a, in_b = row < per, row < 2 * per

    def tile_of(j):
        t = sarr[j].astype(F32)
        fade = jnp.where(in_a, t[3 * per:3 * per + 1], jnp.where(in_b, t[3 * per + 1:3 * per + 2], t[3 * per + 2:3 * per + 3]))
        return t, jnp.exp(fade)

    state = jnp.zeros((mrow, LANES), F32)
    for j in range(nsp):
        t, fade = tile_of(j)
        fsum[j] = state
        state = fade * state + t
    forward = (in_a & low) | (in_b & jnp.logical_not(in_a))
    state = jnp.zeros((mrow, LANES), F32)
    for j in range(nsp - 1, -1, -1):
        t, fade = tile_of(j)
        sret[j] = jnp.where(forward, fsum[j], state).astype(BF16)
        state = fade * state + t
    arrive = send_sp(1, sret, sback, 1)

    z = iota((LANES, nsp * mrow), 0)
    m = iota((LANES, nsp * mrow), 1)
    lift = (z // per) * mrow + z % per
    unpack = [jnp.where(m == lift + g * per, 1.0, 0.0).astype(BF16) for g in range(3)]

    for copy in second:
        copy.wait()
    experts = iota((nsp, toks), 0)
    hits = [jnp.where(rt[k:k + 1] == experts, 1.0, 0.0) for k in range(2)]
    before = jnp.where(r < s, 1.0, 0.0).astype(BF16)
    counts = mm((hits[0] + hits[1]).astype(BF16), before)
    places = [
        rt[k:k + 1] * cap + jnp.sum(hits[k] * counts, axis=0, keepdims=True).astype(jnp.int32) for k in range(2)
    ]

    arrive()
    back = sback[...].reshape(nsp * mrow, LANES)
    come = [mm(unpack[g], back) for g in range(3)]
    fwd_a, back_a = chained(0, up, come[0])[0], chained(0, down, come[0])[0]
    fwd_b, back_b = chained(1, up, come[1])[0], chained(2, down, come[2])[0]
    for b in range(blocks):
        at = slice(b * BLK, (b + 1) * BLK)
        one = mixed[0, at] + mm_t(qin[0, at], jnp.where(low, fwd_a[b], back_a[b]).astype(BF16))
        other = mixed[1, at] + mm_t(qin[1, at], fwd_b[b].astype(BF16)) + mm_t(qin[2, at], back_b[b].astype(BF16))
        done = []
        for value, gate in ((one, g1), (other, g2)):
            normed = value * lax.rsqrt(jnp.mean(value * value, axis=-1, keepdims=True) + 1e-06) * hg[...]
            done.append((normed * jax.nn.silu(gate[at].astype(F32))).astype(BF16))
        for n in range(BLK // own_rows):
            d = b * (BLK // own_rows) + n
            for k in range(2):
                heads[d % 2, d // 2, :, k * LANES:(k + 1) * LANES] = done[k][n * own_rows:(n + 1) * own_rows]

    shared = push(heads.at[1 - c], heads_in, sib_send.at[3], sib_recv.at[3], sib)
    piece = width // 4
    mine = heads[c].reshape(ny * own_rows, 2 * LANES)
    for n in range(4):
        at = slice(n * piece, (n + 1) * piece)
        part[:, :, at] = mm(mine, own_proj[:, at]).reshape(ny, own_rows, piece)
    for copy in lend[:2]:
        copy.wait_recv()
    shared.wait_recv()
    theirs = heads_in[...].reshape(ny * own_rows, 2 * LANES)
    for n in range(4):
        at = slice(n * piece, (n + 1) * piece)
        part[:, :, at] = part[:, :, at] + mm(theirs, other_proj[:, at]).reshape(ny, own_rows, piece)

    chains = ((1, 0, 0), (-1, 1, 0), (1, 1, 1), (-1, 0, 1))

    def chip(step):
        return lax.rem(y + step + ny, ny)

    def at_chip(place):
        return (sp, 2 * place + c)

    hw = width // 2
    sent = {}
    for t in range(half_way):
        for n, (way, chunk, skip) in enumerate(chains):
            h = t + skip
            if h >= half_way:
                continue
            at = slice(chunk * hw, (chunk + 1) * hw)
            total = part[chip(way * (half_way - h)), :, at]
            if t > 0:
                sent[n].wait_recv()
                total = total + parr[n, h - 1].astype(F32)
            pbuf[n, h] = total.astype(BF16)
            sent[n] = push(pbuf.at[n, h], parr.at[n, h], p_send.at[n, h], p_recv.at[n, h], at_chip(chip(way)))
    halves = []
    for chunk in range(2):
        total = part[y, :, chunk * hw:(chunk + 1) * hw]
        for n, (way, of, skip) in enumerate(chains):
            if of == chunk:
                sent[n].wait_recv()
                total = total + parr[n, half_way - 1].astype(F32)
        halves.append(total)
    attn = jnp.concatenate(halves, axis=1).astype(BF16).astype(F32)
    steady = layer_norm(stream[...].astype(F32) + attn, gm[...])
    settled[...] = steady
    msend[...] = steady.astype(BF16)

    def lanes_of(k):
        return pl.ds(pl.multiple_of(k * LANES, LANES), LANES)

    def rows_at(k):
        return pl.ds(pl.multiple_of(k * own_rows, own_rows), own_rows)

    def over_tp(base, src_of, dst):
        for k in range(1, ntp):
            to = lax.rem(tp + k, ntp)
            yield push(src_of(to), dst, t_send.at[base, k], t_recv.at[base, k], (sp, to))

    moved = list(over_tp(0, lambda to: msend.at[:, lanes_of(to)], cols.at[rows_at(tp)]))
    cols[rows_at(tp)] = msend[:, lanes_of(tp)]
    slots = iota((nrow, toks), 0)
    named = [slots == places[k] for k in range(2)]
    gather = jnp.where(named[0] | named[1], 1.0, 0.0).astype(BF16)
    for copy in moved:
        copy.wait_recv()
    dsend[...] = mm(gather, cols[...]).astype(BF16).reshape(nrow // 8, 8, LANES)
    arrive = send_sp(2, dsend, darr, cap // 8)

    share = af[0:1] + af[1:2]
    scaled = jnp.where(named[0], af[0:1] / share, 0.0) + jnp.where(named[1], af[1:2] / share, 0.0)
    scaled = scaled.T
    high = scaled.astype(BF16)
    pick_hi[...] = high
    pick_lo[...] = (scaled - high.astype(F32)).astype(BF16)

    arrive()
    rows[tp] = darr[...].reshape(nrow, LANES)

    def half(k):
        return slice(k * hrow, (k + 1) * hrow)

    def slot(place, core):
        return 2 * place + core

    def hand_on(n, h, chunk, place):
        at = rows.at[slot(place, c), half(chunk)]
        return push(at, at, f_send.at[n, h], f_recv.at[n, h], sib)

    def grow_acc(place, core, chunk, fresh=False):
        k = slot(place, core)
        w = wgu[pl.ds(pl.multiple_of(k * LANES, LANES), LANES)]
        more = mm(rows[k, half(chunk)], w)
        acc[half(chunk)] = more if fresh else acc[half(chunk)] + more

    def ring(n, h):
        way, chunk, skip = chains[n]
        at = rows.at[slot(chip(-way * h), c), half(chunk)]
        return push(at, at, g_send.at[n, h], g_recv.at[n, h], at_chip(chip(way)))

    link = {n: ring(n, 0) for n in range(4)}
    passed = [(hand_on(4, chunk, chunk, y), y, chunk) for chunk in range(2)]
    for chunk in range(2):
        grow_acc(y, c, chunk, fresh=True)
    for h in range(half_way):
        fresh = []
        for n, (way, chunk, skip) in enumerate(chains):
            if h >= half_way - skip:
                continue
            link[n].wait_recv()
            if h + 1 < half_way - skip:
                link[n] = ring(n, h + 1)
            place = chip(-way * (h + 1))
            fresh.append((hand_on(n, h, chunk, place), place, chunk))
        for copy, place, chunk in passed:
            copy.wait_recv()
            grow_acc(place, 1 - c, chunk)
        for copy, place, chunk in fresh:
            grow_acc(place, c, chunk)
        passed = fresh
    for copy, place, chunk in passed:
        copy.wait_recv()
        grow_acc(place, 1 - c, chunk)

    swap = []
    for chunk in range(2):
        at = half(chunk)
        act[at] = (jax.nn.silu(acc[at, 0:LANES]) * acc[at, LANES:2 * LANES]).astype(BF16)
        swap.append(push(act.at[at], act_in.at[at], sib_send.at[4 + chunk], sib_recv.at[4 + chunk], sib))
    lend[2].wait_recv()
    for copy in swap:
        copy.wait_recv()

    def own_part(place, chunk):
        at = lanes_of(slot(place, c))
        return mm(act[half(chunk)], own_down[:, at]) + mm(act_in[half(chunk)], other_down[:, at])

    sent = {}
    for t in range(half_way):
        for n, (way, chunk, skip) in enumerate(chains):
            h = t + skip
            if h >= half_way:
                continue
            total = own_part(chip(way * (half_way - h)), chunk)
            if t > 0:
                sent[n].wait_recv()
                total = total + rarr[n, h - 1].astype(F32)
            rbuf[n, h] = total.astype(BF16)
            sent[n] = push(rbuf.at[n, h], rarr.at[n, h], r_send.at[n, h], r_recv.at[n, h], at_chip(chip(way)))
    for chunk in range(2):
        total = own_part(y, chunk)
        for n, (way, of, skip) in enumerate(chains):
            if of == chunk:
                sent[n].wait_recv()
                total = total + rarr[n, half_way - 1].astype(F32)
        rsend[chunk * hrow // 8:(chunk + 1) * hrow // 8] = total.astype(BF16).reshape(hrow // 8, 8, LANES)
    send_sp(3, rsend, rback, cap // 8)()

    back = rback[...].reshape(nrow, LANES)
    term[...] = (mm(pick_hi[...], back) + mm(pick_lo[...], back)).astype(BF16)
    moved = list(over_tp(1, lambda to: term.at[rows_at(to)], mix.at[:, lanes_of(tp)]))
    mix[:, lanes_of(tp)] = term[rows_at(tp)]
    for copy in moved:
        copy.wait_recv()
    out[...] = layer_norm(settled[...] + mix[...].astype(F32), go[...]).astype(BF16)

    for wait in pending:
        wait()
    for copy in remote:
        copy.wait_send()


def layer(nsp, ntp, *args):
    (q1, k1, v1, g1, d1, q2, k2, v2, g2, d2, hg, p1, p2, st, gm, go, rt, af, eg, eu, ed) = args
    toks = q1.shape[0]
    width = st.shape[1]
    own_rows = toks // ntp
    cap = 3 * toks * 2 // (2 * nsp)
    nrow = nsp * cap
    ny = ntp // 2
    steps = ny // 2
    per = LANES // nsp
    mrow = -(-(3 * per + 3) // 16) * 16
    V = pltpu.VMEM
    D = pltpu.SemaphoreType.DMA
    one = (hg.reshape(1, -1), gm.reshape(1, -1), go.reshape(1, -1), rt.T, af.T)
    operands = (q1, k1, v1, g1, d1, q2, k2, v2, g2, d2, one[0], p1, p2, st, one[1], one[2], one[3], one[4], eg, eu, ed)
    scratch = [
        V(q1.shape, BF16), V(k1.shape, BF16), V(v1.shape, BF16), V(g1.shape, BF16), V(d1.shape, F32),
        V(q2.shape, BF16), V(k2.shape, BF16), V(v2.shape, BF16), V(g2.shape, BF16), V(d2.shape, F32),
        V((1, LANES), F32), V((2 * LANES, width), BF16), V((2 * LANES, width), BF16), V((own_rows, width), BF16),
        V((1, width), F32), V((1, width), F32), V((2, toks), jnp.int32), V((2, toks), F32),
        V((width, 2 * LANES), BF16), V((LANES, width), BF16), V((LANES, width), BF16),
        V((nsp, mrow, LANES), BF16), V((nsp, mrow, LANES), BF16), V((nsp, mrow, LANES), F32),
        V((nsp, mrow, LANES), BF16), V((nsp, mrow, LANES), BF16),
        V((3, toks, LANES), BF16), V((3, toks, LANES), BF16), V((3, toks // BLK, LANES, LANES), F32),
        V((2, toks, LANES), F32), V((2, ny, own_rows, 2 * LANES), BF16), V((ny, own_rows, 2 * LANES), BF16),
        V((ny, own_rows, width), F32),
        V((4, steps, own_rows, width // 2), BF16), V((4, steps, own_rows, width // 2), BF16),
        V((own_rows, width), F32), V((own_rows, width), BF16), V((toks, LANES), BF16),
        V((nrow // 8, 8, LANES), BF16), V((nrow // 8, 8, LANES), BF16), V((ntp, nrow, LANES), BF16),
        V((nrow, 2 * LANES), F32), V((nrow, LANES), BF16), V((nrow, LANES), BF16),
        V((4, steps, nrow // 2, LANES), BF16), V((4, steps, nrow // 2, LANES), BF16),
        V((nrow // 8, 8, LANES), BF16), V((nrow // 8, 8, LANES), BF16),
        V((toks, nrow), BF16), V((toks, nrow), BF16), V((toks, LANES), BF16), V((own_rows, width), BF16),
        D((21,)), D((4 * nsp,)), D((4 * nsp,)), D((6,)), D((6,)), D((4, steps)), D((4, steps)), D((2, ntp)), D((2, ntp)),
        D((4, steps)), D((4, steps)), D((5, max(steps, 2))), D((5, max(steps, 2))), D((4, steps)), D((4, steps)),
    ]
    return pl.pallas_call(
        functools.partial(kernel, (nsp, ntp, toks, cap)),
        out_shape=jax.ShapeDtypeStruct((own_rows, width), BF16),
        in_specs=[pl.BlockSpec(memory_space=ANY)] * len(operands),
        out_specs=pl.BlockSpec(memory_space=pltpu.VMEM),
        scratch_shapes=scratch,
        compiler_params=pltpu.CompilerParams(collective_id=0, has_side_effects=True, vmem_limit_bytes=60 * 1024 * 1024),
        name="layer",
    )(*operands)


def solution(mesh):
    spec = P("sp", "tp")
    fade = P(None, "sp", "tp")
    return jax.shard_map(
        functools.partial(layer, mesh.shape["sp"], mesh.shape["tp"]),
        mesh=mesh,
        in_specs=(
            spec, spec, spec, spec, fade, spec, spec, spec, spec, fade,
            P(), P("tp", None), P("tp", None), P("sp", None), P(), P(), P("sp", None), P("sp", None),
            P("sp", None, "tp"), P("sp", None, "tp"), P("sp", "tp", None),
        ),
        out_specs=P(("sp", "tp"), None),
        check_vma=False,
    )
```

time: 403 us -> 123 us (0.31)
  blocking collectives: 174 us -> 0 us
  Pallas kernels: 0 us -> 118 us
  waiting for transfers between devices: 114 us -> 0 us
  starting transfers between devices: 35.3 us -> 0 us
  other arithmetic: 25.8 us -> 0 us
  matrix products: 20.4 us -> 0 us
  between operations: 14.9 us -> 0.01 us
  local copies, waits for them, and re-layouts: 17.7 us -> 5.31 us
    pallas_call x0 -> x1, Pallas kernels: none -> 118 us  [layer(): pl.pallas_call(functools.partial(kernel, (nsp, ntp, toks, cap)), out_shap...]
    all_to_all x3 -> x0, blocking collectives: 109 us -> none  [the longest x1 77.5 us: summed_on_arrival(): lax.all_to_all(pieces, axis, split_axis=0, concat_axis=0, tiled=True)]
    all_gather x2 -> x0, waiting for transfers between devices: 74.4 us -> none  [the longest x1 42.4 us: body(): complete = lax.all_gather(arrived, 'tp', axis=3, tiled=True)]
    all_gather x4 -> x0, blocking collectives: 65 us -> none  [gathered_once(): both, at, found = (lax.all_gather(jnp.concatenate(lines), axis), 0, {})]
    all_to_all x2 -> x0, waiting for transfers between devices: 39.4 us -> none  [the longest x1 27.9 us: summed_on_arrival(): lax.all_to_all(pieces, axis, split_axis=0, concat_axis=0, tiled=True)]
    all_to_all x2 -> x0, starting transfers between devices: 35.1 us -> none  [the longest x1 25.2 us: summed_on_arrival(): lax.all_to_all(pieces, axis, split_axis=0, concat_axis=0, tiled=True)]
    dot_general x20 -> x0, matrix products: 20.4 us -> none  [the longest x1 6.95 us: body(): jnp.einsum('secf,efd->secd', act, expert_down, preferred_element_type=jnp...]
    reduce_sum x9 -> x0, other arithmetic: 7.02 us -> none  [the longest x2 3.2 us: summed_on_arrival(): return arrived.astype(jnp.float32).sum(axis=0)]
  transfers between devices with their start and end apart: 4 -> 0, of which waited for: 4 -> 0; matrix products, arithmetic and copies ran while one was open for 1% -> 0% of each run, Pallas kernels for 0% -> 0%
where the time goes in v1:
time: 123 us
  Pallas kernels  118 us (96%)
  local copies, waits for them, and re-layouts  5.31 us (4%)
    pallas_call x1, Pallas kernels, layer(): pl.pallas_call(functools.partial(kernel, (nsp, ntp, toks, cap)), out_shap...  118 us
    unnamed x6, local copies, waits for them, and re-layouts  5.31 us

profile of v1, /device:TPU:1, one launch (start us, length us, event | category | flops | bytes accessed | tf_op | source)
XLA Modules:
  0.0 123.0 jit_solution(12308084156655370291)
XLA Ops:
  0.0 0.0 copy-start
  0.0 1.5 %copy.22.q1h = bf16[256,64]{1,0:T(8,128)(2,1)} copy(bf16[256,64]{0,1:T(8,128)(2,1)} %param.21) | data formatting | bytes 65536 | tf_op args[0]
  1.5 1.5 %copy.23.k1h = bf16[256,64]{1,0:T(8,128)(2,1)} copy(bf16[256,64]{0,1:T(8,128)(2,1)} %param.22) | data formatting | bytes 65536 | tf_op args[1]
  3.0 0.0 copy-done
  3.0 0.8 copy.24.d1h
  3.8 117.6 %layer.1 = bf16[16,2048]{1,0:T(8,128)(2,1)} custom-call(bf16[256,64]{1,0:T(8,128)(2,1)} %copy.22.q1h, bf16[256,64]{1,0:T(8,128)(2,1)} %copy.23.k1h, bf16[256,128]{1,0:T(8,128)(2,1)} %v1h.1, bf16[256,128]{1,0:T(8,128)(2,1)} %g1h.1, f32[2,256,64]{2,1,0:T(8,128)} %copy.24.d1h, bf16[256,128]{1,0:T(8,128)(2,1)} %q2h.1, bf16[256,128]{1,0:T(8,128)(2,1)} %k2h.1, ...), custom_call_target="tpu_custom_call" | custom-call | tf_op jit(solution)/shard_map/layer/pallas_call | solution.py:494
  121.5 1.5 %copy.26 = bf16[16,2048]{1,0:T(8,128)(2,1)} copy(bf16[16,2048]{1,0:T(8,128)(2,1)} %layer.1) | data formatting | bytes 131072
Async XLA Ops:
  0.0 3.0 %copy-start = (f32[2,256,64]{1,2,0:T(8,128)S(1)}, f32[2,256,64]{1,2,0:T(8,128)}, u32[]{:S(2)}) copy-start(f32[2,256,64]{1,2,0:T(8,128)} %param.25) | copy-start | bytes 393220

commit v2 on v1

v2 whole, which is shorter than its diff:
```python
import functools

import jax
import jax.numpy as jnp
from jax import lax
from jax.experimental import pallas as pl
from jax.experimental.pallas import tpu as pltpu
from jax.sharding import PartitionSpec as P

MESH = pl.DeviceIdType.MESH
F32 = jnp.float32
BF16 = jnp.bfloat16
BLK = 64
CHUNKS = 4
LANES = 128
ANY = pl.ANY


def mm(a, b):
    return jnp.dot(a, b, preferred_element_type=F32)


def mm_t(a, b):
    return lax.dot_general(a, b, (((1,), (1,)), ((), ())), preferred_element_type=F32)


def tmm(a, b):
    return lax.dot_general(a, b, (((0,), (0,)), ((), ())), preferred_element_type=F32)


def iota(shape, dim):
    return lax.broadcasted_iota(jnp.int32, shape, dim)


def far_first(sizes):
    steps = [()]
    for size in sizes:
        steps = [done + (k,) for done in steps for k in range(size)]
    return sorted(steps, key=lambda d: (-sum(min(k, n - k) for k, n in zip(d, sizes)), d))


def layer_norm(values, gain):
    mean = jnp.mean(values, axis=-1, keepdims=True)
    spread = jnp.mean(jnp.square(values - mean), axis=-1, keepdims=True)
    return (values - mean) * lax.rsqrt(spread + 1e-05) * gain


def kernel(
    cfg,
    q1h, k1h, v1h, g1h, d1h, q2h, k2h, v2h, g2h, d2h, hgh, p1h, p2h, sth, gmh, goh, rth, afh, egh, euh, edh,
    out,
    q1, k1, v1, g1, d1, q2, k2, v2, g2, d2, hg, own_proj, other_proj, stream, gm, go, rt, af, wgu, down,
    sbuf, sarr, fsum, sret, sback,
    qin, kin, grow, mixed, heads, heads_in, part,
    pbuf, parr, settled, msend, cols, dsend, darr, rows, acc, act, rbuf, rarr, rsend, rback,
    pick_hi, pick_lo, term, mix,
    load_sem, s_send, s_recv, sib_send, sib_recv, p_send, p_recv, t_send, t_recv,
    g_send, g_recv, f_send, f_recv, r_send, r_recv,
):
    nsp, nx, ntp, toks, cap = cfg
    nz = nsp // nx
    ny = ntp // 2
    half_way = ny // 2
    sp = lax.axis_index("sp")
    tp = lax.axis_index("tp")
    y = lax.div(tp, 2)
    c = lax.rem(tp, 2)
    sib = (sp, tp + 1 - 2 * c)
    blocks = toks // BLK
    own_rows = toks // ntp
    width = ntp * LANES
    per = LANES // nsp
    mrow = sbuf.shape[1]
    nrow = nsp * cap
    crow = nrow // CHUNKS
    z_at, x_at = lax.div(sp, nx), lax.rem(sp, nx)
    sp_moves = far_first((nz, nx))
    tp_moves = far_first((ny, 2))

    scope = []

    def phase(name):
        if scope:
            scope.pop().__exit__(None, None, None)
        if name:
            scope.append(jax.named_scope(name))
            scope[0].__enter__()

    phase("greet")
    barrier = pltpu.get_barrier_semaphore()

    def greet_sp(k, carry):
        pl.semaphore_signal(barrier, inc=1, device_id=(lax.rem(sp + k, nsp), tp), device_id_type=MESH)
        return carry

    def greet_tp(k, carry):
        pl.semaphore_signal(barrier, inc=1, device_id=(sp, lax.rem(tp + k, ntp)), device_id_type=MESH)
        return carry

    lax.fori_loop(1, nsp, greet_sp, 0)
    lax.fori_loop(1, ntp, greet_tp, 0)

    loads = []

    def load(src, dst):
        copy = pltpu.make_async_copy(src, dst, load_sem.at[len(loads)])
        copy.start()
        loads.append(copy)
        return copy

    first = [load(a, b) for a, b in ((d1h, d1), (d2h, d2), (k1h, k1), (v1h, v1), (k2h, k2), (v2h, v2), (q1h, q1), (q2h, q2))]
    second = [
        load(a, b)
        for a, b in (
            (g1h, g1), (g2h, g2), (hgh, hg), (p1h, own_proj.at[0:LANES]), (p2h, own_proj.at[LANES:2 * LANES]),
            (sth.at[pl.ds(pl.multiple_of(tp * own_rows, own_rows), own_rows)], stream), (gmh, gm), (goh, go),
            (rth, rt), (afh, af),
            (egh.at[0], wgu.at[:, 0:LANES]), (euh.at[0], wgu.at[:, LANES:2 * LANES]), (edh.at[0], down.at[0:LANES]),
        )
    ]

    phase("constants")
    r = iota((toks, toks), 0)
    s = iota((toks, toks), 1)
    tri = jnp.where((r // BLK == s // BLK) & (s <= r), 1.0, 0.0).astype(BF16)
    low = iota((1, LANES), 1) < LANES // 2
    m = iota((nsp * mrow, LANES), 0)
    o, i = m // mrow, m % mrow
    wanted = jnp.where(i < 3 * per, (i // per) * LANES + o * per + i % per, 3 * LANES + i - 3 * per)
    wanted = jnp.where(i < 3 * per + 3, wanted, -1)
    lane = iota((nsp * mrow, LANES), 1)
    pack = [jnp.where(wanted == lane + g * LANES, 1.0, 0.0).astype(BF16) for g in range(3)]
    lane16 = iota((nsp * mrow, 16), 1)
    pack.append(jnp.where(wanted[:, 0:16] == lane16 + 3 * LANES, 1.0, 0.0).astype(BF16))

    phase("load_wait")
    for copy in first:
        copy.wait()
    phase("fading")

    def two(a):
        a = a[...].astype(F32)
        return jnp.concatenate([a, a], axis=0).T

    fading = (d1[...].T, d2[0], d2[1])
    keys = (two(k1), k2[...].astype(F32), k2[...].astype(F32))
    queries = (two(q1) * 64 ** (-0.5), q2[...].astype(F32) * 128 ** (-0.5), q2[...].astype(F32) * 128 ** (-0.5))
    values = (v1[...], v2[...], v2[...])
    totals = []
    for g in range(3):
        x = fading[g]
        logs = (jnp.minimum(x, 0.0) - jnp.log1p(jnp.exp(-jnp.abs(x)))) * (1.0 / 16.0)
        hi = logs.astype(BF16)
        rest = logs - hi.astype(F32)
        mid = rest.astype(BF16)
        lo = (rest - mid.astype(F32)).astype(BF16)
        cum = mm(tri, hi) + mm(tri, mid) + mm(tri, lo)
        rows_of = []
        for b in range(blocks):
            at = slice(b * BLK, (b + 1) * BLK)
            ahead = cum[at]
            tot = ahead[BLK - 1:BLK]
            behind = tot - ahead + logs[at]
            run = ahead if g == 1 else behind if g == 2 else jnp.where(low, ahead, behind)
            qin[g, at] = (queries[g][at] * jnp.exp(run)).astype(BF16)
            kin[g, at] = (keys[g][at] * jnp.exp(-run)).astype(BF16)
            kst = (keys[g][at] * jnp.exp(tot - run)).astype(BF16)
            grow[g, b] = tmm(values[g][at], kst)
            rows_of.append(tot)
        totals.append(rows_of)

    fades = [[jnp.exp(t) for t in row] for row in totals]

    def chained(g, order, start):
        state = start
        seen = {}
        for b in order:
            seen[b] = state
            state = fades[g][b] * state + grow[g, b]
        return seen, state

    phase("chain")
    rise, fall = list(range(blocks)), list(range(blocks - 1, -1, -1))
    zero = jnp.zeros((LANES, LANES), F32)
    ends = [
        jnp.where(low, chained(0, rise, zero)[1], chained(0, fall, zero)[1]),
        chained(1, rise, zero)[1],
        chained(2, fall, zero)[1],
    ]
    sums = [sum(row[1:], row[0]) for row in totals]
    r16 = iota((16, LANES), 0)
    tail = jnp.where(r16 == 0, sums[0], jnp.where(r16 == 1, sums[1], jnp.where(r16 == 2, sums[2], 0.0)))
    packed = mm(pack[3], tail.astype(BF16))
    for g in range(3):
        packed = packed + mm(pack[g], ends[g].astype(BF16))
    sbuf[...] = packed.astype(BF16).reshape(nsp, mrow, LANES)

    phase("barrier")
    pl.semaphore_wait(barrier, nsp - 1 + ntp - 1)

    unsent = []

    def sp_peer(move, way):
        return lax.rem(z_at + way * move[0] + nz, nz) * nx + lax.rem(x_at + way * move[1] + nx, nx)

    def send_sp(base, p, src, dst, way=1):
        copy = pltpu.make_async_remote_copy(
            src, dst, s_send.at[base * nsp + p], s_recv.at[base * nsp + p],
            device_id=(sp_peer(sp_moves[p], way), tp), device_id_type=MESH,
        )
        copy.start()
        unsent.append(copy)
        return copy

    def drain():
        while unsent:
            unsent.pop(0).wait_send()

    def push(src, dst, ssem, rsem, device):
        copy = pltpu.make_async_remote_copy(src, dst, ssem, rsem, device_id=device, device_id_type=MESH)
        copy.start()
        unsent.append(copy)
        return copy

    phase("send_states")
    coming = [send_sp(0, p, sbuf.at[sp_peer(sp_moves[p], 1)], sarr.at[sp]) for p in range(nsp - 1)]
    sarr[sp] = sbuf[sp]
    lend = [
        push(p1h, other_proj.at[0:LANES], sib_send.at[0], sib_recv.at[0], sib),
        push(p2h, other_proj.at[LANES:2 * LANES], sib_send.at[1], sib_recv.at[1], sib),
        push(edh.at[0], down.at[LANES:2 * LANES], sib_send.at[2], sib_recv.at[2], sib),
        push(egh.at[0], wgu.at[:, 2 * LANES:3 * LANES], sib_send.at[4], sib_recv.at[4], sib),
        push(euh.at[0], wgu.at[:, 3 * LANES:4 * LANES], sib_send.at[5], sib_recv.at[5], sib),
    ]

    phase("inner")
    rr, cc = iota((BLK, BLK), 0), iota((BLK, BLK), 1)
    lower, upper = cc <= rr, cc >= rr
    for b in range(blocks):
        at = slice(b * BLK, (b + 1) * BLK)
        q, k = qin[0, at], kin[0, at]
        nil = jnp.zeros_like(q)
        score = jnp.where(lower, mm_t(jnp.where(low, q, nil), k), 0.0) + jnp.where(upper, mm_t(jnp.where(low, nil, q), k), 0.0)
        mixed[0, at] = mm(score.astype(BF16), values[0][at])
        score = jnp.where(lower, mm_t(qin[1, at], kin[1, at]), 0.0) + jnp.where(upper, mm_t(qin[2, at], kin[2, at]), 0.0)
        mixed[1, at] = mm(score.astype(BF16), values[1][at])

    phase("wait_states")
    for copy in coming:
        copy.wait_recv()
    phase("scan")
    row = iota((mrow, LANES), 0)
    in_a, in_b = row < per, row < 2 * per

    def tile_of(j):
        t = sarr[j].astype(F32)
        fade = jnp.where(in_a, t[3 * per:3 * per + 1], jnp.where(in_b, t[3 * per + 1:3 * per + 2], t[3 * per + 2:3 * per + 3]))
        return t, jnp.exp(fade)

    state = jnp.zeros((mrow, LANES), F32)
    for j in range(nsp):
        t, fade = tile_of(j)
        fsum[j] = state
        state = fade * state + t
    forward = (in_a & low) | (in_b & jnp.logical_not(in_a))
    state = jnp.zeros((mrow, LANES), F32)
    for j in range(nsp - 1, -1, -1):
        t, fade = tile_of(j)
        sret[j] = jnp.where(forward, fsum[j], state).astype(BF16)
        state = fade * state + t
    phase("send_back")
    coming = [send_sp(1, p, sret.at[sp_peer(sp_moves[p], 1)], sback.at[sp]) for p in range(nsp - 1)]
    sback[sp] = sret[sp]

    phase("places")
    z = iota((LANES, nsp * mrow), 0)
    m = iota((LANES, nsp * mrow), 1)
    lift = (z // per) * mrow + z % per
    unpack = [jnp.where(m == lift + g * per, 1.0, 0.0).astype(BF16) for g in range(3)]

    for copy in second:
        copy.wait()
    experts = iota((nsp, toks), 0)
    hits = [jnp.where(rt[k:k + 1] == experts, 1.0, 0.0) for k in range(2)]
    before = jnp.where(r < s, 1.0, 0.0).astype(BF16)
    counts = mm((hits[0] + hits[1]).astype(BF16), before)
    places = [
        rt[k:k + 1] * cap + jnp.sum(hits[k] * counts, axis=0, keepdims=True).astype(jnp.int32) for k in range(2)
    ]

    phase("wait_back")
    for copy in coming:
        copy.wait_recv()
    phase("readout")
    back = sback[...].reshape(nsp * mrow, LANES)
    come = [mm(unpack[g], back) for g in range(3)]
    fwd_a, back_a = chained(0, rise, come[0])[0], chained(0, fall, come[0])[0]
    fwd_b, back_b = chained(1, rise, come[1])[0], chained(2, fall, come[2])[0]
    for b in range(blocks):
        at = slice(b * BLK, (b + 1) * BLK)
        one = mixed[0, at] + mm_t(qin[0, at], jnp.where(low, fwd_a[b], back_a[b]).astype(BF16))
        other = mixed[1, at] + mm_t(qin[1, at], fwd_b[b].astype(BF16)) + mm_t(qin[2, at], back_b[b].astype(BF16))
        done = []
        for value, gate in ((one, g1), (other, g2)):
            normed = value * lax.rsqrt(jnp.mean(value * value, axis=-1, keepdims=True) + 1e-06) * hg[...]
            done.append((normed * jax.nn.silu(gate[at].astype(F32))).astype(BF16))
        for n in range(BLK // own_rows):
            d = b * (BLK // own_rows) + n
            for k in range(2):
                heads[d % 2, d // 2, :, k * LANES:(k + 1) * LANES] = done[k][n * own_rows:(n + 1) * own_rows]

    phase("proj")
    shared = push(heads.at[1 - c], heads_in, sib_send.at[3], sib_recv.at[3], sib)
    piece = width // 4
    mine = heads[c].reshape(ny * own_rows, 2 * LANES)
    for n in range(4):
        at = slice(n * piece, (n + 1) * piece)
        part[:, :, at] = mm(mine, own_proj[:, at]).reshape(ny, own_rows, piece)
    for copy in lend[:2]:
        copy.wait_recv()
    shared.wait_recv()
    theirs = heads_in[...].reshape(ny * own_rows, 2 * LANES)
    for n in range(4):
        at = slice(n * piece, (n + 1) * piece)
        part[:, :, at] = part[:, :, at] + mm(theirs, other_proj[:, at]).reshape(ny, own_rows, piece)

    phase("attn_ring")
    chains = [(way, q, (q % 2 == 0) != (way == 1)) for q in range(CHUNKS) for way in (1, -1)]
    chain_no = {(way, q): n for n, (way, q, skip) in enumerate(chains)}

    def chip(step):
        return lax.rem(y + step + ny, ny)

    def at_chip(place):
        return (sp, 2 * place + c)

    wide = width // CHUNKS
    sent = {}
    for t in range(half_way):
        for n, (way, q, skip) in enumerate(chains):
            h = t + skip
            if h >= half_way:
                continue
            total = part[chip(way * (half_way - h)), :, q * wide:(q + 1) * wide]
            if t > 0:
                sent[n].wait_recv()
                total = total + parr[n, h - 1].astype(F32)
            pbuf[n, h] = total.astype(BF16)
            sent[n] = push(pbuf.at[n, h], parr.at[n, h], p_send.at[n, h], p_recv.at[n, h], at_chip(chip(way)))
    quarters = []
    for q in range(CHUNKS):
        total = part[y, :, q * wide:(q + 1) * wide]
        for way in (1, -1):
            n = chain_no[way, q]
            if n in sent:
                sent[n].wait_recv()
                total = total + parr[n, half_way - 1].astype(F32)
        quarters.append(total)
    phase("norm")
    attn = jnp.concatenate(quarters, axis=1).astype(BF16).astype(F32)
    steady = layer_norm(stream[...].astype(F32) + attn, gm[...])
    settled[...] = steady
    msend[...] = steady.astype(BF16)

    phase("rows_over_tp")

    def lanes_of(k):
        return pl.ds(pl.multiple_of(k * LANES, LANES), LANES)

    def rows_at(k):
        return pl.ds(pl.multiple_of(k * own_rows, own_rows), own_rows)

    def over_tp(base, src_of, dst):
        copies = []
        for p, (dy, dc) in enumerate(tp_moves[:-1]):
            to = 2 * chip(dy) + (lax.rem(c + dc, 2))
            copies.append(push(src_of(to), dst, t_send.at[base, p], t_recv.at[base, p], (sp, to)))
        return copies

    moved = over_tp(0, lambda to: msend.at[:, lanes_of(to)], cols.at[rows_at(tp)])
    cols[rows_at(tp)] = msend[:, lanes_of(tp)]
    slots = iota((nrow, toks), 0)
    named = [slots == places[k] for k in range(2)]
    gather = jnp.where(named[0] | named[1], 1.0, 0.0).astype(BF16)
    phase("rows_wait")
    for copy in moved:
        copy.wait_recv()
    phase("dispatch")
    dsend[...] = mm(gather, cols[...]).astype(BF16).reshape(nrow // 8, 8, LANES)
    unit = cap // 8
    rows_of_peer = lambda k: pl.ds(k * unit, unit)
    coming = [
        send_sp(2, p, dsend.at[rows_of_peer(sp_peer(sp_moves[p], 1))], darr.at[p * unit:(p + 1) * unit])
        for p in range(nsp - 1)
    ]
    darr[(nsp - 1) * unit:nsp * unit] = dsend[rows_of_peer(sp)]

    phase("weights")
    drain()
    share = af[0:1] + af[1:2]
    scaled = jnp.where(named[0], af[0:1] / share, 0.0) + jnp.where(named[1], af[1:2] / share, 0.0)
    scaled = scaled.T
    high = scaled.astype(BF16)
    pick_hi[...] = high
    pick_lo[...] = (scaled - high.astype(F32)).astype(BF16)

    phase("dispatch_wait")

    def chunk(q):
        return slice(q * crow, (q + 1) * crow)

    def slot(place, core):
        return 2 * place + core

    def hand_on(n, h, q, place):
        at = rows.at[slot(place, c), chunk(q)]
        return push(at, at, f_send.at[n, h], f_recv.at[n, h], sib)

    def ring(n, h):
        way, q, skip = chains[n]
        at = rows.at[slot(chip(-way * h), c), chunk(q)]
        return push(at, at, g_send.at[n, h], g_recv.at[n, h], at_chip(chip(way)))

    def grow_acc(copy, q, place, fresh=False):
        copy.wait_recv()
        both = jnp.concatenate([rows[slot(place, 0), chunk(q)], rows[slot(place, 1), chunk(q)]], axis=1)
        more = mm(both, wgu[pl.ds(pl.multiple_of(place * 2 * LANES, 2 * LANES), 2 * LANES)])
        acc[chunk(q)] = more if fresh else acc[chunk(q)] + more

    link, passed = {}, []
    peers = nsp // CHUNKS
    for q in range(CHUNKS):
        for p in range(q * nsp // CHUNKS, (q + 1) * nsp // CHUNKS):
            if p < nsp - 1:
                coming[p].wait_recv()
        rows[tp, chunk(q)] = darr[q * crow // 8:(q + 1) * crow // 8].reshape(crow, LANES)
        for way in (1, -1):
            n = chain_no[way, q]
            if half_way - chains[n][2] > 0:
                link[n] = ring(n, 0)
        passed.append((hand_on(len(chains), q, q, y), q, y, True))
    phase("gather_ring")
    for copy in lend[2:]:
        copy.wait_recv()
    for h in range(half_way - 1):
        fresh = []
        for n, (way, q, skip) in enumerate(chains):
            if h >= half_way - skip:
                continue
            link[n].wait_recv()
            if h + 1 < half_way - skip:
                link[n] = ring(n, h + 1)
            place = chip(-way * (h + 1))
            fresh.append((hand_on(n, h, q, place), q, place))
        for item in passed:
            grow_acc(*item)
        passed = fresh
    for item in passed:
        grow_acc(*item)

    def last_piece(q):
        way = 1 if q % 2 == 0 else -1
        n = chain_no[way, q]
        link[n].wait_recv()
        place = chip(half_way)
        return hand_on(n, half_way - 1, q, place), q, place

    def own_part(place, q):
        return mm(act[chunk(q)], down[:, lanes_of(slot(place, c))])

    sent = {}

    def reduce_step(n, t):
        way, q, skip = chains[n]
        h = t + skip
        if h >= half_way:
            return
        total = own_part(chip(way * (half_way - h)), q)
        if t > 0:
            sent[n].wait_recv()
            total = total + rarr[n, h - 1].astype(F32)
        rbuf[n, h] = total.astype(BF16)
        sent[n] = push(rbuf.at[n, h], rarr.at[n, h], r_send.at[n, h], r_recv.at[n, h], at_chip(chip(way)))

    def finish_rows(item):
        grow_acc(*item)
        q = item[1]
        a = acc[chunk(q)]
        for k in range(2):
            gate, up = a[:, 2 * k * LANES:(2 * k + 1) * LANES], a[:, (2 * k + 1) * LANES:(2 * k + 2) * LANES]
            act[chunk(q), k * LANES:(k + 1) * LANES] = (jax.nn.silu(gate) * up).astype(BF16)
        for way in (1, -1):
            reduce_step(chain_no[way, q], 0)

    drain()
    phase("last_pieces")
    waiting = [last_piece(0)]
    for q in range(1, CHUNKS):
        waiting.append(last_piece(q))
        finish_rows(waiting[q - 1])
    finish_rows(waiting[CHUNKS - 1])
    phase("reduce_ring")
    for t in range(1, half_way):
        for n in range(len(chains)):
            reduce_step(n, t)
    coming = []
    for q in range(CHUNKS):
        total = own_part(y, q)
        for way in (1, -1):
            n = chain_no[way, q]
            if n in sent:
                sent[n].wait_recv()
                total = total + rarr[n, half_way - 1].astype(F32)
        rsend[q * crow // 8:(q + 1) * crow // 8] = total.astype(BF16).reshape(crow // 8, 8, LANES)
        for p in range(q * nsp // CHUNKS, (q + 1) * nsp // CHUNKS):
            if p < nsp - 1:
                coming.append(send_sp(3, p, rsend.at[p * unit:(p + 1) * unit], rback.at[rows_of_peer(sp)], -1))
    rback[rows_of_peer(sp)] = rsend[(nsp - 1) * unit:nsp * unit]
    phase("return_wait")
    drain()
    for copy in coming:
        copy.wait_recv()
    phase("combine")

    back = rback[...].reshape(nrow, LANES)
    term[...] = (mm(pick_hi[...], back) + mm(pick_lo[...], back)).astype(BF16)
    phase("mix_over_tp")
    moved = over_tp(1, lambda to: term.at[rows_at(to)], mix.at[:, lanes_of(tp)])
    mix[:, lanes_of(tp)] = term[rows_at(tp)]
    for copy in moved:
        copy.wait_recv()
    phase("last_norm")
    out[...] = layer_norm(settled[...] + mix[...].astype(F32), go[...]).astype(BF16)

    phase("drain")
    drain()
    phase(None)


def layer(nsp, ntp, *args):
    (q1, k1, v1, g1, d1, q2, k2, v2, g2, d2, hg, p1, p2, st, gm, go, rt, af, eg, eu, ed) = args
    toks = q1.shape[0]
    width = st.shape[1]
    own_rows = toks // ntp
    cap = 3 * toks * 2 // (2 * nsp)
    nrow = nsp * cap
    ny = ntp // 2
    steps = ny // 2
    per = LANES // nsp
    mrow = -(-(3 * per + 3) // 16) * 16
    V = pltpu.VMEM
    D = pltpu.SemaphoreType.DMA
    one = (hg.reshape(1, -1), gm.reshape(1, -1), go.reshape(1, -1), rt.T, af.T)
    q1, k1 = q1.T, k1.T
    d1 = d1.transpose(0, 2, 1).reshape(2 * q1.shape[0], toks)
    operands = (q1, k1, v1, g1, d1, q2, k2, v2, g2, d2, one[0], p1, p2, st, one[1], one[2], one[3], one[4], eg, eu, ed)
    scratch = [
        V(q1.shape, BF16), V(k1.shape, BF16), V(v1.shape, BF16), V(g1.shape, BF16), V(d1.shape, F32),
        V(q2.shape, BF16), V(k2.shape, BF16), V(v2.shape, BF16), V(g2.shape, BF16), V(d2.shape, F32),
        V((1, LANES), F32), V((2 * LANES, width), BF16), V((2 * LANES, width), BF16), V((own_rows, width), BF16),
        V((1, width), F32), V((1, width), F32), V((2, toks), jnp.int32), V((2, toks), F32),
        V((width, 4 * LANES), BF16), V((2 * LANES, width), BF16),
        V((nsp, mrow, LANES), BF16), V((nsp, mrow, LANES), BF16), V((nsp, mrow, LANES), F32),
        V((nsp, mrow, LANES), BF16), V((nsp, mrow, LANES), BF16),
        V((3, toks, LANES), BF16), V((3, toks, LANES), BF16), V((3, toks // BLK, LANES, LANES), F32),
        V((2, toks, LANES), F32), V((2, ny, own_rows, 2 * LANES), BF16), V((ny, own_rows, 2 * LANES), BF16),
        V((ny, own_rows, width), F32),
        V((2 * CHUNKS, steps, own_rows, width // CHUNKS), BF16), V((2 * CHUNKS, steps, own_rows, width // CHUNKS), BF16),
        V((own_rows, width), F32), V((own_rows, width), BF16), V((toks, LANES), BF16),
        V((nrow // 8, 8, LANES), BF16), V((nrow // 8, 8, LANES), BF16), V((ntp, nrow, LANES), BF16),
        V((nrow, 4 * LANES), F32), V((nrow, 2 * LANES), BF16),
        V((2 * CHUNKS, steps, nrow // CHUNKS, LANES), BF16), V((2 * CHUNKS, steps, nrow // CHUNKS, LANES), BF16),
        V((nrow // 8, 8, LANES), BF16), V((nrow // 8, 8, LANES), BF16),
        V((toks, nrow), BF16), V((toks, nrow), BF16), V((toks, LANES), BF16), V((own_rows, width), BF16),
        D((21,)), D((4 * nsp,)), D((4 * nsp,)), D((6,)), D((6,)), D((2 * CHUNKS, steps)), D((2 * CHUNKS, steps)),
        D((2, ntp)), D((2, ntp)), D((2 * CHUNKS, steps)), D((2 * CHUNKS, steps)),
        D((2 * CHUNKS + 1, max(steps, CHUNKS))), D((2 * CHUNKS + 1, max(steps, CHUNKS))),
        D((2 * CHUNKS, steps)), D((2 * CHUNKS, steps)),
    ]
    return pl.pallas_call(
        functools.partial(kernel, (nsp, 4 if nsp % 4 == 0 else 1, ntp, toks, cap)),
        out_shape=jax.ShapeDtypeStruct((own_rows, width), BF16),
        in_specs=[pl.BlockSpec(memory_space=ANY)] * len(operands),
        out_specs=pl.BlockSpec(memory_space=pltpu.VMEM),
        scratch_shapes=scratch,
        compiler_params=pltpu.CompilerParams(collective_id=0, has_side_effects=True, vmem_limit_bytes=60 * 1024 * 1024),
        name="layer",
    )(*operands)


def solution(mesh):
    spec = P("sp", "tp")
    fade = P(None, "sp", "tp")
    return jax.shard_map(
        functools.partial(layer, mesh.shape["sp"], mesh.shape["tp"]),
        mesh=mesh,
        in_specs=(
            spec, spec, spec, spec, fade, spec, spec, spec, spec, fade,
            P(), P("tp", None), P("tp", None), P("sp", None), P(), P(), P("sp", None), P("sp", None),
            P("sp", None, "tp"), P("sp", None, "tp"), P("sp", "tp", None),
        ),
        out_specs=P(("sp", "tp"), None),
        check_vma=False,
    )
```

time: 123 us -> 112 us (0.911)
  Pallas kernels: 118 us -> 110 us
  local copies, waits for them, and re-layouts: 5.31 us -> 1.47 us
    pallas_call x1, Pallas kernels: 118 us -> 110 us  [layer(): pl.pallas_call(functools.partial(kernel, (nsp, 4 if nsp % 4 == 0 else 1,...]
    unnamed x6 -> x1, local copies, waits for them, and re-layouts: 5.31 us -> 1.47 us
where the time goes in v2:
time: 112 us; the launch traced here: 111 us
  Pallas kernels  110 us (98%)
  local copies, waits for them, and re-layouts  1.47 us (1%)
    pallas_call x1, Pallas kernels, layer(): pl.pallas_call(functools.partial(kernel, (nsp, 4 if nsp % 4 == 0 else 1,...  110 us

profile of v2, /device:TPU:1, one launch (start us, length us, event | category | flops | bytes accessed | tf_op | source)
XLA Modules:
  0.0 111.4 jit_solution(10249093182433136631)
XLA Ops:
  0.0 109.9 %layer.1 = bf16[16,2048]{1,0:T(8,128)(2,1)} custom-call(bf16[64,256]{1,0:T(8,128)(2,1)} %bitcast.11, bf16[64,256]{1,0:T(8,128)(2,1)} %bitcast.12, bf16[256,128]{1,0:T(8,128)(2,1)} %v1h.1, bf16[256,128]{1,0:T(8,128)(2,1)} %g1h.1, f32[128,256]{1,0:T(8,128)} %bitcast.10, bf16[256,128]{1,0:T(8,128)(2,1)} %q2h.1, bf16[256,128]{1,0:T(8,128)(2,1)} %k2h.1, ...), custom_call_target="tpu_custom_call" | custom-call | tf_op jit(solution)/shard_map/layer/pallas_call | solution.py:580
  109.9 1.5 %copy.23 = bf16[16,2048]{1,0:T(8,128)(2,1)} copy(bf16[16,2048]{1,0:T(8,128)(2,1)} %layer.1) | data formatting | bytes 131072

commit v3 on v2

--- a/solution.py
+++ b/solution.py
@@ -49,13 +49,12 @@
     cfg,
     q1h, k1h, v1h, g1h, d1h, q2h, k2h, v2h, g2h, d2h, hgh, p1h, p2h, sth, gmh, goh, rth, afh, egh, euh, edh,
     out,
-    q1, k1, v1, g1, d1, q2, k2, v2, g2, d2, hg, own_proj, other_proj, stream, gm, go, rt, af, wgu, down,
+    qk1, wide_in, gates, d1, d2, hg, own_proj, other_proj, stream, gains, rt, af, wgu, down,
     sbuf, sarr, fsum, sret, sback,
     qin, kin, grow, mixed, heads, heads_in, part,
     pbuf, parr, settled, msend, cols, dsend, darr, rows, acc, act, rbuf, rarr, rsend, rback,
     pick_hi, pick_lo, term, mix,
-    load_sem, s_send, s_recv, sib_send, sib_recv, p_send, p_recv, t_send, t_recv,
-    g_send, g_recv, f_send, f_recv, r_send, r_recv,
+    sems,
 ):
     nsp, nx, ntp, toks, cap = cfg
     nz = nsp // nx
@@ -77,6 +76,15 @@
     sp_moves = far_first((nz, nx))
     tp_moves = far_first((ny, 2))
 
+    def sp_peer(move, way):
+        return lax.rem(z_at + way * move[0] + nz, nz) * nx + lax.rem(x_at + way * move[1] + nx, nx)
+
+    def chip(step):
+        return lax.rem(y + step + ny, ny)
+
+    def tp_peer(move):
+        return 2 * chip(move[0]) + lax.rem(c + move[1], 2)
+
     scope = []
 
     def phase(name):
@@ -86,37 +94,39 @@
             scope.append(jax.named_scope(name))
             scope[0].__enter__()
 
+    numbers = iter(range(sems.shape[0]))
+
+    def new_sem():
+        return sems.at[next(numbers)]
+
+    def await_bytes(ref, sem):
+        pltpu.make_async_copy(ref, ref, sem).wait()
+
+    def load(*pairs):
+        sem = new_sem()
+        for src, dst in pairs:
+            pltpu.make_async_copy(src, dst, sem).start()
+        return sem
+
     phase("greet")
+    first = [
+        (d1, load((d1h, d1))), (d2, load((d2h, d2))),
+        (wide_in, load((k2h, wide_in.at[0]), (v1h, wide_in.at[1]), (v2h, wide_in.at[2]), (q2h, wide_in.at[3]))),
+        (qk1, load((q1h, qk1.at[0]), (k1h, qk1.at[1]))),
+    ]
     barrier = pltpu.get_barrier_semaphore()
-
-    def greet_sp(k, carry):
-        pl.semaphore_signal(barrier, inc=1, device_id=(lax.rem(sp + k, nsp), tp), device_id_type=MESH)
-        return carry
-
-    def greet_tp(k, carry):
-        pl.semaphore_signal(barrier, inc=1, device_id=(sp, lax.rem(tp + k, ntp)), device_id_type=MESH)
-        return carry
-
-    lax.fori_loop(1, nsp, greet_sp, 0)
-    lax.fori_loop(1, ntp, greet_tp, 0)
-
-    loads = []
-
-    def load(src, dst):
-        copy = pltpu.make_async_copy(src, dst, load_sem.at[len(loads)])
-        copy.start()
-        loads.append(copy)
-        return copy
-
-    first = [load(a, b) for a, b in ((d1h, d1), (d2h, d2), (k1h, k1), (v1h, v1), (k2h, k2), (v2h, v2), (q1h, q1), (q2h, q2))]
+    for move in sp_moves[:-1]:
+        pl.semaphore_signal(barrier, inc=1, device_id=(sp_peer(move, 1), tp), device_id_type=MESH)
+    for move in tp_moves[:-1]:
+        pl.semaphore_signal(barrier, inc=1, device_id=(sp, tp_peer(move)), device_id_type=MESH)
+    own_stream = sth.at[pl.ds(pl.multiple_of(tp * own_rows, own_rows), own_rows)]
     second = [
-        load(a, b)
-        for a, b in (
-            (g1h, g1), (g2h, g2), (hgh, hg), (p1h, own_proj.at[0:LANES]), (p2h, own_proj.at[LANES:2 * LANES]),
-            (sth.at[pl.ds(pl.multiple_of(tp * own_rows, own_rows), own_rows)], stream), (gmh, gm), (goh, go),
-            (rth, rt), (afh, af),
-            (egh.at[0], wgu.at[:, 0:LANES]), (euh.at[0], wgu.at[:, LANES:2 * LANES]), (edh.at[0], down.at[0:LANES]),
-        )
+        (gates, load((g1h, gates.at[0]), (g2h, gates.at[1]))), (hg, load((hgh, hg))),
+        (own_proj, load((p1h, own_proj.at[0:LANES]), (p2h, own_proj.at[LANES:2 * LANES]))),
+        (stream, load((own_stream, stream))), (gains, load((gmh, gains.at[0:1]), (goh, gains.at[1:2]))),
+        (rt, load((rth, rt))), (af, load((afh, af))),
+        (wgu.at[:, 0:2 * LANES], load((egh.at[0], wgu.at[:, 0:LANES]), (euh.at[0], wgu.at[:, LANES:2 * LANES]))),
+        (down.at[0:LANES], load((edh.at[0], down.at[0:LANES]))),
     ]
 
     phase("constants")
@@ -134,18 +144,18 @@
     pack.append(jnp.where(wanted[:, 0:16] == lane16 + 3 * LANES, 1.0, 0.0).astype(BF16))
 
     phase("load_wait")
-    for copy in first:
-        copy.wait()
+    for item in first:
+        await_bytes(*item)
     phase("fading")
 
     def two(a):
-        a = a[...].astype(F32)
+        a = a.astype(F32)
         return jnp.concatenate([a, a], axis=0).T
 
     fading = (d1[...].T, d2[0], d2[1])
-    keys = (two(k1), k2[...].astype(F32), k2[...].astype(F32))
-    queries = (two(q1) * 64 ** (-0.5), q2[...].astype(F32) * 128 ** (-0.5), q2[...].astype(F32) * 128 ** (-0.5))
-    values = (v1[...], v2[...], v2[...])
+    keys = (two(qk1[1]), wide_in[0].astype(F32), wide_in[0].astype(F32))
+    queries = (two(qk1[0]) * 64 ** (-0.5), wide_in[3].astype(F32) * 128 ** (-0.5), wide_in[3].astype(F32) * 128 ** (-0.5))
+    values = (wide_in[1], wide_in[2], wide_in[2])
     totals = []
     for g in range(3):
         x = fading[g]
@@ -198,40 +208,41 @@
     phase("barrier")
     pl.semaphore_wait(barrier, nsp - 1 + ntp - 1)
 
-    unsent = []
-
-    def sp_peer(move, way):
-        return lax.rem(z_at + way * move[0] + nz, nz) * nx + lax.rem(x_at + way * move[1] + nx, nx)
-
-    def send_sp(base, p, src, dst, way=1):
-        copy = pltpu.make_async_remote_copy(
-            src, dst, s_send.at[base * nsp + p], s_recv.at[base * nsp + p],
-            device_id=(sp_peer(sp_moves[p], way), tp), device_id_type=MESH,
-        )
-        copy.start()
-        unsent.append(copy)
-        return copy
+    left = []
+
+    def push(src, dst, ssem, rsem, device):
+        pltpu.make_async_remote_copy(src, dst, ssem, rsem, device_id=device, device_id_type=MESH).start()
+
+    def lend(size, *pairs):
+        ssem, rsem = new_sem(), new_sem()
+        for src, dst in pairs:
+            push(src, dst, ssem, rsem, sib)
+        left.append((size, ssem))
+        return size, rsem
 
     def drain():
-        while unsent:
-            unsent.pop(0).wait_send()
-
-    def push(src, dst, ssem, rsem, device):
-        copy = pltpu.make_async_remote_copy(src, dst, ssem, rsem, device_id=device, device_id_type=MESH)
-        copy.start()
-        unsent.append(copy)
-        return copy
+        while left:
+            await_bytes(*left.pop(0))
+
+    def to_sp(p, way=1):
+        return (sp_peer(sp_moves[p], way), tp)
 
     phase("send_states")
-    coming = [send_sp(0, p, sbuf.at[sp_peer(sp_moves[p], 1)], sarr.at[sp]) for p in range(nsp - 1)]
-    sarr[sp] = sbuf[sp]
-    lend = [
-        push(p1h, other_proj.at[0:LANES], sib_send.at[0], sib_recv.at[0], sib),
-        push(p2h, other_proj.at[LANES:2 * LANES], sib_send.at[1], sib_recv.at[1], sib),
-        push(edh.at[0], down.at[LANES:2 * LANES], sib_send.at[2], sib_recv.at[2], sib),
-        push(egh.at[0], wgu.at[:, 2 * LANES:3 * LANES], sib_send.at[4], sib_recv.at[4], sib),
-        push(euh.at[0], wgu.at[:, 3 * LANES:4 * LANES], sib_send.at[5], sib_recv.at[5], sib),
-    ]
+    def over_sp(src, dst):
+        ssem, rsem = new_sem(), new_sem()
+        for p in range(nsp - 1):
+            to = to_sp(p)
+            push(src.at[to[0]], dst.at[sp], ssem, rsem, to)
+        left.append((src.at[0:nsp - 1], ssem))
+        dst[sp] = src[sp]
+        return dst.at[0:nsp - 1], rsem
+
+    coming = over_sp(sbuf, sarr)
+    lent_proj = lend(other_proj, (p1h, other_proj.at[0:LANES]), (p2h, other_proj.at[LANES:2 * LANES]))
+    lent_wgu = lend(
+        wgu.at[:, 2 * LANES:4 * LANES], (egh.at[0], wgu.at[:, 2 * LANES:3 * LANES]), (euh.at[0], wgu.at[:, 3 * LANES:4 * LANES])
+    )
+    lent_down = lend(down.at[LANES:2 * LANES], (edh.at[0], down.at[LANES:2 * LANES]))
 
     phase("inner")
     rr, cc = iota((BLK, BLK), 0), iota((BLK, BLK), 1)
@@ -246,8 +257,7 @@
         mixed[1, at] = mm(score.astype(BF16), values[1][at])
 
     phase("wait_states")
-    for copy in coming:
-        copy.wait_recv()
+    await_bytes(*coming)
     phase("scan")
     row = iota((mrow, LANES), 0)
     in_a, in_b = row < per, row < 2 * per
@@ -269,8 +279,7 @@
         sret[j] = jnp.where(forward, fsum[j], state).astype(BF16)
         state = fade * state + t
     phase("send_back")
-    coming = [send_sp(1, p, sret.at[sp_peer(sp_moves[p], 1)], sback.at[sp]) for p in range(nsp - 1)]
-    sback[sp] = sret[sp]
+    coming = over_sp(sret, sback)
 
     phase("places")
     z = iota((LANES, nsp * mrow), 0)
@@ -278,8 +287,8 @@
     lift = (z // per) * mrow + z % per
     unpack = [jnp.where(m == lift + g * per, 1.0, 0.0).astype(BF16) for g in range(3)]
 
-    for copy in second:
-        copy.wait()
+    for item in second:
+        await_bytes(*item)
     experts = iota((nsp, toks), 0)
     hits = [jnp.where(rt[k:k + 1] == experts, 1.0, 0.0) for k in range(2)]
     before = jnp.where(r < s, 1.0, 0.0).astype(BF16)
@@ -289,8 +298,7 @@
     ]
 
     phase("wait_back")
-    for copy in coming:
-        copy.wait_recv()
+    await_bytes(*coming)
     phase("readout")
     back = sback[...].reshape(nsp * mrow, LANES)
     come = [mm(unpack[g], back) for g in range(3)]
@@ -301,7 +309,7 @@
         one = mixed[0, at] + mm_t(qin[0, at], jnp.where(low, fwd_a[b], back_a[b]).astype(BF16))
         other = mixed[1, at] + mm_t(qin[1, at], fwd_b[b].astype(BF16)) + mm_t(qin[2, at], back_b[b].astype(BF16))
         done = []
-        for value, gate in ((one, g1), (other, g2)):
+        for value, gate in ((one, gates.at[0]), (other, gates.at[1])):
             normed = value * lax.rsqrt(jnp.mean(value * value, axis=-1, keepdims=True) + 1e-06) * hg[...]
             done.append((normed * jax.nn.silu(gate[at].astype(F32))).astype(BF16))
         for n in range(BLK // own_rows):
@@ -310,15 +318,14 @@
                 heads[d % 2, d // 2, :, k * LANES:(k + 1) * LANES] = done[k][n * own_rows:(n + 1) * own_rows]
 
     phase("proj")
-    shared = push(heads.at[1 - c], heads_in, sib_send.at[3], sib_recv.at[3], sib)
+    shared = lend(heads_in, (heads.at[1 - c], heads_in))
     piece = width // 4
     mine = heads[c].reshape(ny * own_rows, 2 * LANES)
     for n in range(4):
         at = slice(n * piece, (n + 1) * piece)
         part[:, :, at] = mm(mine, own_proj[:, at]).reshape(ny, own_rows, piece)
-    for copy in lend[:2]:
-        copy.wait_recv()
-    shared.wait_recv()
+    await_bytes(*lent_proj)
+    await_bytes(*shared)
     theirs = heads_in[...].reshape(ny * own_rows, 2 * LANES)
     for n in range(4):
         at = slice(n * piece, (n + 1) * piece)
@@ -328,14 +335,11 @@
     chains = [(way, q, (q % 2 == 0) != (way == 1)) for q in range(CHUNKS) for way in (1, -1)]
     chain_no = {(way, q): n for n, (way, q, skip) in enumerate(chains)}
 
-    def chip(step):
-        return lax.rem(y + step + ny, ny)
-
     def at_chip(place):
         return (sp, 2 * place + c)
 
     wide = width // CHUNKS
-    sent = {}
+    sent, pieces, all_sent = {}, 0, new_sem()
     for t in range(half_way):
         for n, (way, q, skip) in enumerate(chains):
             h = t + skip
@@ -343,22 +347,25 @@
                 continue
             total = part[chip(way * (half_way - h)), :, q * wide:(q + 1) * wide]
             if t > 0:
-                sent[n].wait_recv()
+                await_bytes(parr.at[n, h - 1], sent[n])
                 total = total + parr[n, h - 1].astype(F32)
             pbuf[n, h] = total.astype(BF16)
-            sent[n] = push(pbuf.at[n, h], parr.at[n, h], p_send.at[n, h], p_recv.at[n, h], at_chip(chip(way)))
+            sent[n] = new_sem()
+            push(pbuf.at[n, h], parr.at[n, h], all_sent, sent[n], at_chip(chip(way)))
+            pieces += 1
     quarters = []
     for q in range(CHUNKS):
         total = part[y, :, q * wide:(q + 1) * wide]
         for way in (1, -1):
             n = chain_no[way, q]
             if n in sent:
-                sent[n].wait_recv()
+                await_bytes(parr.at[n, half_way - 1], sent[n])
                 total = total + parr[n, half_way - 1].astype(F32)
         quarters.append(total)
+    left.append((pbuf.at[0:pieces // half_way], all_sent))
     phase("norm")
     attn = jnp.concatenate(quarters, axis=1).astype(BF16).astype(F32)
-    steady = layer_norm(stream[...].astype(F32) + attn, gm[...])
+    steady = layer_norm(stream[...].astype(F32) + attn, gains[0:1])
     settled[...] = steady
     msend[...] = steady.astype(BF16)
 
@@ -370,29 +377,35 @@
     def rows_at(k):
         return pl.ds(pl.multiple_of(k * own_rows, own_rows), own_rows)
 
-    def over_tp(base, src_of, dst):
-        copies = []
-        for p, (dy, dc) in enumerate(tp_moves[:-1]):
-            to = 2 * chip(dy) + (lax.rem(c + dc, 2))
-            copies.append(push(src_of(to), dst, t_send.at[base, p], t_recv.at[base, p], (sp, to)))
-        return copies
-
-    moved = over_tp(0, lambda to: msend.at[:, lanes_of(to)], cols.at[rows_at(tp)])
+    def over_tp(src_of, dst):
+        ssem, rsem = new_sem(), new_sem()
+        for move in tp_moves[:-1]:
+            to = tp_peer(move)
+            push(src_of(to), dst, ssem, rsem, (sp, to))
+        size = cols.at[0:(ntp - 1) * own_rows]
+        left.append((size, ssem))
+        return size, rsem
+
+    moved = over_tp(lambda to: msend.at[:, lanes_of(to)], cols.at[rows_at(tp)])
     cols[rows_at(tp)] = msend[:, lanes_of(tp)]
     slots = iota((nrow, toks), 0)
     named = [slots == places[k] for k in range(2)]
     gather = jnp.where(named[0] | named[1], 1.0, 0.0).astype(BF16)
     phase("rows_wait")
-    for copy in moved:
-        copy.wait_recv()
+    await_bytes(*moved)
     phase("dispatch")
     dsend[...] = mm(gather, cols[...]).astype(BF16).reshape(nrow // 8, 8, LANES)
     unit = cap // 8
     rows_of_peer = lambda k: pl.ds(k * unit, unit)
-    coming = [
-        send_sp(2, p, dsend.at[rows_of_peer(sp_peer(sp_moves[p], 1))], darr.at[p * unit:(p + 1) * unit])
-        for p in range(nsp - 1)
-    ]
+    all_sent, coming = new_sem(), []
+    for q in range(CHUNKS):
+        span = range(q * nsp // CHUNKS, min((q + 1) * nsp // CHUNKS, nsp - 1))
+        rsem = new_sem()
+        for p in span:
+            to = to_sp(p)
+            push(dsend.at[rows_of_peer(to[0])], darr.at[p * unit:(p + 1) * unit], all_sent, rsem, to)
+        coming.append((darr.at[span[0] * unit:(span[-1] + 1) * unit], rsem) if span else None)
+    left.append((dsend.at[0:(nsp - 1) * unit], all_sent))
     darr[(nsp - 1) * unit:nsp * unit] = dsend[rows_of_peer(sp)]
 
     phase("weights")
@@ -412,46 +425,53 @@
     def slot(place, core):
         return 2 * place + core
 
-    def hand_on(n, h, q, place):
+    ring_sent, hand_sent = new_sem(), new_sem()
+    counts_of = [0, 0]
+
+    def hand_on(q, place):
         at = rows.at[slot(place, c), chunk(q)]
-        return push(at, at, f_send.at[n, h], f_recv.at[n, h], sib)
+        rsem = new_sem()
+        push(at, at, hand_sent, rsem, sib)
+        counts_of[1] += 1
+        return rows.at[slot(place, 1 - c), chunk(q)], rsem
 
     def ring(n, h):
         way, q, skip = chains[n]
         at = rows.at[slot(chip(-way * h), c), chunk(q)]
-        return push(at, at, g_send.at[n, h], g_recv.at[n, h], at_chip(chip(way)))
+        rsem = new_sem()
+        push(at, at, ring_sent, rsem, at_chip(chip(way)))
+        counts_of[0] += 1
+        return rows.at[slot(chip(-way * (h + 1)), c), chunk(q)], rsem
 
     def grow_acc(copy, q, place, fresh=False):
-        copy.wait_recv()
+        await_bytes(*copy)
         both = jnp.concatenate([rows[slot(place, 0), chunk(q)], rows[slot(place, 1), chunk(q)]], axis=1)
         more = mm(both, wgu[pl.ds(pl.multiple_of(place * 2 * LANES, 2 * LANES), 2 * LANES)])
         acc[chunk(q)] = more if fresh else acc[chunk(q)] + more
 
     link, passed = {}, []
-    peers = nsp // CHUNKS
     for q in range(CHUNKS):
-        for p in range(q * nsp // CHUNKS, (q + 1) * nsp // CHUNKS):
-            if p < nsp - 1:
-                coming[p].wait_recv()
+        if coming[q]:
+            await_bytes(*coming[q])
         rows[tp, chunk(q)] = darr[q * crow // 8:(q + 1) * crow // 8].reshape(crow, LANES)
         for way in (1, -1):
             n = chain_no[way, q]
             if half_way - chains[n][2] > 0:
                 link[n] = ring(n, 0)
-        passed.append((hand_on(len(chains), q, q, y), q, y, True))
+        passed.append((hand_on(q, y), q, y, True))
     phase("gather_ring")
-    for copy in lend[2:]:
-        copy.wait_recv()
+    await_bytes(*lent_wgu)
+    await_bytes(*lent_down)
     for h in range(half_way - 1):
         fresh = []
         for n, (way, q, skip) in enumerate(chains):
             if h >= half_way - skip:
                 continue
-            link[n].wait_recv()
+            await_bytes(*link[n])
             if h + 1 < half_way - skip:
                 link[n] = ring(n, h + 1)
             place = chip(-way * (h + 1))
-            fresh.append((hand_on(n, h, q, place), q, place))
+            fresh.append((hand_on(q, place), q, place))
         for item in passed:
             grow_acc(*item)
         passed = fresh
@@ -461,14 +481,14 @@
     def last_piece(q):
         way = 1 if q % 2 == 0 else -1
         n = chain_no[way, q]
-        link[n].wait_recv()
+        await_bytes(*link[n])
         place = chip(half_way)
-        return hand_on(n, half_way - 1, q, place), q, place
+        return hand_on(q, place), q, place
 
     def own_part(place, q):
         return mm(act[chunk(q)], down[:, lanes_of(slot(place, c))])
 
-    sent = {}
+    sent, reduced, all_sent = {}, [0], new_sem()
 
     def reduce_step(n, t):
         way, q, skip = chains[n]
@@ -477,10 +497,12 @@
             return
         total = own_part(chip(way * (half_way - h)), q)
         if t > 0:
-            sent[n].wait_recv()
+            await_bytes(rarr.at[n, h - 1], sent[n])
             total = total + rarr[n, h - 1].astype(F32)
         rbuf[n, h] = total.astype(BF16)
-        sent[n] = push(rbuf.at[n, h], rarr.at[n, h], r_send.at[n, h], r_recv.at[n, h], at_chip(chip(way)))
+        sent[n] = new_sem()
+        push(rbuf.at[n, h], rarr.at[n, h], all_sent, sent[n], at_chip(chip(way)))
+        reduced[0] += 1
 
     def finish_rows(item):
         grow_acc(*item)
@@ -503,34 +525,35 @@
     for t in range(1, half_way):
         for n in range(len(chains)):
             reduce_step(n, t)
-    coming = []
+    left.append((rbuf.at[0:reduced[0] // half_way], all_sent))
+    left.append((rows.at[0:counts_of[0] // CHUNKS], ring_sent))
+    left.append((rows.at[0:counts_of[1] // CHUNKS], hand_sent))
+    all_sent, arrived = new_sem(), new_sem()
     for q in range(CHUNKS):
         total = own_part(y, q)
         for way in (1, -1):
             n = chain_no[way, q]
             if n in sent:
-                sent[n].wait_recv()
+                await_bytes(rarr.at[n, half_way - 1], sent[n])
                 total = total + rarr[n, half_way - 1].astype(F32)
         rsend[q * crow // 8:(q + 1) * crow // 8] = total.astype(BF16).reshape(crow // 8, 8, LANES)
-        for p in range(q * nsp // CHUNKS, (q + 1) * nsp // CHUNKS):
-            if p < nsp - 1:
-                coming.append(send_sp(3, p, rsend.at[p * unit:(p + 1) * unit], rback.at[rows_of_peer(sp)], -1))
+        for p in range(q * nsp // CHUNKS, min((q + 1) * nsp // CHUNKS, nsp - 1)):
+            push(rsend.at[p * unit:(p + 1) * unit], rback.at[rows_of_peer(sp)], all_sent, arrived, to_sp(p, -1))
+    left.append((rsend.at[0:(nsp - 1) * unit], all_sent))
     rback[rows_of_peer(sp)] = rsend[(nsp - 1) * unit:nsp * unit]
     phase("return_wait")
     drain()
-    for copy in coming:
-        copy.wait_recv()
+    await_bytes(rback.at[0:(nsp - 1) * unit], arrived)
     phase("combine")
 
     back = rback[...].reshape(nrow, LANES)
     term[...] = (mm(pick_hi[...], back) + mm(pick_lo[...], back)).astype(BF16)
     phase("mix_over_tp")
-    moved = over_tp(1, lambda to: term.at[rows_at(to)], mix.at[:, lanes_of(tp)])
+    moved = over_tp(lambda to: term.at[rows_at(to)], mix.at[:, lanes_of(tp)])
     mix[:, lanes_of(tp)] = term[rows_at(tp)]
-    for copy in moved:
-        copy.wait_recv()
+    await_bytes(*moved)
     phase("last_norm")
-    out[...] = layer_norm(settled[...] + mix[...].astype(F32), go[...]).astype(BF16)
+    out[...] = layer_norm(settled[...] + mix[...].astype(F32), gains[1:2]).astype(BF16)
 
     phase("drain")
     drain()
@@ -555,10 +578,9 @@
     d1 = d1.transpose(0, 2, 1).reshape(2 * q1.shape[0], toks)
     operands = (q1, k1, v1, g1, d1, q2, k2, v2, g2, d2, one[0], p1, p2, st, one[1], one[2], one[3], one[4], eg, eu, ed)
     scratch = [
-        V(q1.shape, BF16), V(k1.shape, BF16), V(v1.shape, BF16), V(g1.shape, BF16), V(d1.shape, F32),
-        V(q2.shape, BF16), V(k2.shape, BF16), V(v2.shape, BF16), V(g2.shape, BF16), V(d2.shape, F32),
+        V((2, *q1.shape), BF16), V((4, *q2.shape), BF16), V((2, *q2.shape), BF16), V(d1.shape, F32), V(d2.shape, F32),
         V((1, LANES), F32), V((2 * LANES, width), BF16), V((2 * LANES, width), BF16), V((own_rows, width), BF16),
-        V((1, width), F32), V((1, width), F32), V((2, toks), jnp.int32), V((2, toks), F32),
+        V((2, width), F32), V((2, toks), jnp.int32), V((2, toks), F32),
         V((width, 4 * LANES), BF16), V((2 * LANES, width), BF16),
         V((nsp, mrow, LANES), BF16), V((nsp, mrow, LANES), BF16), V((nsp, mrow, LANES), F32),
         V((nsp, mrow, LANES), BF16), V((nsp, mrow, LANES), BF16),
@@ -572,10 +594,7 @@
         V((2 * CHUNKS, steps, nrow // CHUNKS, LANES), BF16), V((2 * CHUNKS, steps, nrow // CHUNKS, LANES), BF16),
         V((nrow // 8, 8, LANES), BF16), V((nrow // 8, 8, LANES), BF16),
         V((toks, nrow), BF16), V((toks, nrow), BF16), V((toks, LANES), BF16), V((own_rows, width), BF16),
-        D((21,)), D((4 * nsp,)), D((4 * nsp,)), D((6,)), D((6,)), D((2 * CHUNKS, steps)), D((2 * CHUNKS, steps)),
-        D((2, ntp)), D((2, ntp)), D((2 * CHUNKS, steps)), D((2 * CHUNKS, steps)),
-        D((2 * CHUNKS + 1, max(steps, CHUNKS))), D((2 * CHUNKS + 1, max(steps, CHUNKS))),
-        D((2 * CHUNKS, steps)), D((2 * CHUNKS, steps)),
+        D((156,)),
     ]
     return pl.pallas_call(
         functools.partial(kernel, (nsp, 4 if nsp % 4 == 0 else 1, ntp, toks, cap)),

time: 112 us -> 107 us (0.955)
  Pallas kernels: 110 us -> 105 us
    pallas_call x1, Pallas kernels: 110 us -> 105 us  [layer(): pl.pallas_call(functools.partial(kernel, (nsp, 4 if nsp % 4 == 0 else 1,...]
where the time goes in v3:
time: 107 us
  Pallas kernels  105 us (98%)
  local copies, waits for them, and re-layouts  1.47 us (1%)
    pallas_call x1, Pallas kernels, layer(): pl.pallas_call(functools.partial(kernel, (nsp, 4 if nsp % 4 == 0 else 1,...  105 us

profile of v3, /device:TPU:1, one launch (start us, length us, event | category | flops | bytes accessed | tf_op | source)
XLA Modules:
  0.0 106.6 jit_solution(17205834042440312284)
XLA Ops:
  0.0 105.1 %layer.1 = bf16[16,2048]{1,0:T(8,128)(2,1)} custom-call(bf16[64,256]{1,0:T(8,128)(2,1)} %bitcast.11, bf16[64,256]{1,0:T(8,128)(2,1)} %bitcast.12, bf16[256,128]{1,0:T(8,128)(2,1)} %v1h.1, bf16[256,128]{1,0:T(8,128)(2,1)} %g1h.1, f32[128,256]{1,0:T(8,128)} %bitcast.10, bf16[256,128]{1,0:T(8,128)(2,1)} %q2h.1, bf16[256,128]{1,0:T(8,128)(2,1)} %k2h.1, ...), custom_call_target="tpu_custom_call" | custom-call | tf_op jit(solution)/shard_map/layer/pallas_call | solution.py:599
  105.1 1.5 %copy.23 = bf16[16,2048]{1,0:T(8,128)(2,1)} copy(bf16[16,2048]{1,0:T(8,128)(2,1)} %layer.1) | data formatting | bytes 131072

commit v4 on v3

--- a/solution.py
+++ b/solution.py
@@ -52,7 +52,7 @@
     qk1, wide_in, gates, d1, d2, hg, own_proj, other_proj, stream, gains, rt, af, wgu, down,
     sbuf, sarr, fsum, sret, sback,
     qin, kin, grow, mixed, heads, heads_in, part,
-    pbuf, parr, settled, msend, cols, dsend, darr, rows, acc, act, rbuf, rarr, rsend, rback,
+    pbuf, parr, settled, settled_cols, own_stats, stats, chosen, xsend, xarr, tilt, cols, dsend, darr, rows, acc, act, rbuf, rarr, rsend, rback,
     pick_hi, pick_lo, term, mix,
     sems,
 ):
@@ -119,7 +119,7 @@
         pl.semaphore_signal(barrier, inc=1, device_id=(sp_peer(move, 1), tp), device_id_type=MESH)
     for move in tp_moves[:-1]:
         pl.semaphore_signal(barrier, inc=1, device_id=(sp, tp_peer(move)), device_id_type=MESH)
-    own_stream = sth.at[pl.ds(pl.multiple_of(tp * own_rows, own_rows), own_rows)]
+    own_stream = sth.at[:, pl.ds(pl.multiple_of(tp * LANES, LANES), LANES)]
     second = [
         (gates, load((g1h, gates.at[0]), (g2h, gates.at[1]))), (hg, load((hgh, hg))),
         (own_proj, load((p1h, own_proj.at[0:LANES]), (p2h, own_proj.at[LANES:2 * LANES]))),
@@ -312,24 +312,27 @@
         for value, gate in ((one, gates.at[0]), (other, gates.at[1])):
             normed = value * lax.rsqrt(jnp.mean(value * value, axis=-1, keepdims=True) + 1e-06) * hg[...]
             done.append((normed * jax.nn.silu(gate[at].astype(F32))).astype(BF16))
-        for n in range(BLK // own_rows):
-            d = b * (BLK // own_rows) + n
-            for k in range(2):
-                heads[d % 2, d // 2, :, k * LANES:(k + 1) * LANES] = done[k][n * own_rows:(n + 1) * own_rows]
+        for k in range(2):
+            heads[at, k * LANES:(k + 1) * LANES] = done[k]
 
     phase("proj")
-    shared = lend(heads_in, (heads.at[1 - c], heads_in))
-    piece = width // 4
-    mine = heads[c].reshape(ny * own_rows, 2 * LANES)
-    for n in range(4):
-        at = slice(n * piece, (n + 1) * piece)
-        part[:, :, at] = mm(mine, own_proj[:, at]).reshape(ny, own_rows, piece)
+    shared = lend(heads_in, (heads, heads_in))
+
+    def lanes_of(k):
+        return pl.ds(pl.multiple_of(k * LANES, LANES), LANES)
+
+    def rows_at(k):
+        return pl.ds(pl.multiple_of(k * own_rows, own_rows), own_rows)
+
+    def slot(place, core):
+        return 2 * place + core
+
+    for d in range(ny):
+        part[d] = mm(heads[...], own_proj[:, lanes_of(slot(d, c))])
     await_bytes(*lent_proj)
     await_bytes(*shared)
-    theirs = heads_in[...].reshape(ny * own_rows, 2 * LANES)
-    for n in range(4):
-        at = slice(n * piece, (n + 1) * piece)
-        part[:, :, at] = part[:, :, at] + mm(theirs, other_proj[:, at]).reshape(ny, own_rows, piece)
+    for d in range(ny):
+        part[d] = part[d] + mm(heads_in[...], other_proj[:, lanes_of(slot(d, c))])
 
     phase("attn_ring")
     chains = [(way, q, (q % 2 == 0) != (way == 1)) for q in range(CHUNKS) for way in (1, -1)]
@@ -338,78 +341,81 @@
     def at_chip(place):
         return (sp, 2 * place + c)
 
-    wide = width // CHUNKS
-    sent, pieces, all_sent = {}, 0, new_sem()
-    for t in range(half_way):
-        for n, (way, q, skip) in enumerate(chains):
-            h = t + skip
-            if h >= half_way:
-                continue
-            total = part[chip(way * (half_way - h)), :, q * wide:(q + 1) * wide]
-            if t > 0:
-                await_bytes(parr.at[n, h - 1], sent[n])
-                total = total + parr[n, h - 1].astype(F32)
-            pbuf[n, h] = total.astype(BF16)
-            sent[n] = new_sem()
-            push(pbuf.at[n, h], parr.at[n, h], all_sent, sent[n], at_chip(chip(way)))
-            pieces += 1
-    quarters = []
+    tall = toks // CHUNKS
+    pieces, all_sent = [0], new_sem()
+
+    def span(q):
+        return slice(q * tall, (q + 1) * tall)
+
+    def toward(n, kind, total, hops):
+        way = chains[n][0]
+        sem = new_sem()
+        pbuf[n, kind] = total.astype(BF16)
+        push(pbuf.at[n, kind], parr.at[n, kind], all_sent, sem, at_chip(chip(way * hops)))
+        pieces[0] += 1
+        return parr.at[n, kind], sem
+
+    def added(total, item):
+        await_bytes(*item)
+        return total + item[0][...].astype(F32)
+
+    third, fourth, near, merged = {}, {}, {}, {}
+    for n, (way, q, skip) in enumerate(chains):
+        third[n] = toward(n, 0, part[chip(3 * way), span(q)], 1)
+        if not skip:
+            fourth[n] = toward(n, 1, part[chip(4 * way), span(q)], 2)
+    for n, (way, q, skip) in enumerate(chains):
+        near[n] = toward(n, 2, part[chip(way), span(q)], 1)
+    for n, (way, q, skip) in enumerate(chains):
+        total = added(part[chip(2 * way), span(q)], third[n])
+        if not skip:
+            total = added(total, fourth[n])
+        merged[n] = toward(n, 3, total, 2)
+    own_gain = gains[0:1, lanes_of(tp)]
     for q in range(CHUNKS):
-        total = part[y, :, q * wide:(q + 1) * wide]
-        for way in (1, -1):
-            n = chain_no[way, q]
-            if n in sent:
-                await_bytes(parr.at[n, half_way - 1], sent[n])
-                total = total + parr[n, half_way - 1].astype(F32)
-        quarters.append(total)
-    left.append((pbuf.at[0:pieces // half_way], all_sent))
-    phase("norm")
-    attn = jnp.concatenate(quarters, axis=1).astype(BF16).astype(F32)
-    steady = layer_norm(stream[...].astype(F32) + attn, gains[0:1])
-    settled[...] = steady
-    msend[...] = steady.astype(BF16)
-
-    phase("rows_over_tp")
-
-    def lanes_of(k):
-        return pl.ds(pl.multiple_of(k * LANES, LANES), LANES)
-
-    def rows_at(k):
-        return pl.ds(pl.multiple_of(k * own_rows, own_rows), own_rows)
-
-    def over_tp(src_of, dst):
+        total = part[y, span(q)]
+        for items in (near, merged):
+            for way in (1, -1):
+                total = added(total, items[chain_no[way, q]])
+        summed = stream[span(q)].astype(F32) + total.astype(BF16).astype(F32)
+        settled_cols[span(q)] = summed
+        cols[span(q)] = ((summed - jnp.mean(summed, axis=-1, keepdims=True)) * own_gain).astype(BF16)
+    left.append((pbuf.at[0:pieces[0] // 4], all_sent))
+    phase("dispatch")
+
+    def over_tp(src_of, dst, size):
         ssem, rsem = new_sem(), new_sem()
         for move in tp_moves[:-1]:
             to = tp_peer(move)
             push(src_of(to), dst, ssem, rsem, (sp, to))
-        size = cols.at[0:(ntp - 1) * own_rows]
         left.append((size, ssem))
         return size, rsem
 
-    moved = over_tp(lambda to: msend.at[:, lanes_of(to)], cols.at[rows_at(tp)])
-    cols[rows_at(tp)] = msend[:, lanes_of(tp)]
     slots = iota((nrow, toks), 0)
     named = [slots == places[k] for k in range(2)]
     gather = jnp.where(named[0] | named[1], 1.0, 0.0).astype(BF16)
-    phase("rows_wait")
-    await_bytes(*moved)
-    phase("dispatch")
+    chosen[...] = gather
     dsend[...] = mm(gather, cols[...]).astype(BF16).reshape(nrow // 8, 8, LANES)
     unit = cap // 8
     rows_of_peer = lambda k: pl.ds(k * unit, unit)
-    all_sent, coming = new_sem(), []
-    for q in range(CHUNKS):
-        span = range(q * nsp // CHUNKS, min((q + 1) * nsp // CHUNKS, nsp - 1))
-        rsem = new_sem()
-        for p in span:
-            to = to_sp(p)
-            push(dsend.at[rows_of_peer(to[0])], darr.at[p * unit:(p + 1) * unit], all_sent, rsem, to)
-        coming.append((darr.at[span[0] * unit:(span[-1] + 1) * unit], rsem) if span else None)
-    left.append((dsend.at[0:(nsp - 1) * unit], all_sent))
-    darr[(nsp - 1) * unit:nsp * unit] = dsend[rows_of_peer(sp)]
-
+
+    def to_experts(src, dst):
+        all_sent, coming = new_sem(), []
+        for q in range(CHUNKS):
+            some = range(q * nsp // CHUNKS, min((q + 1) * nsp // CHUNKS, nsp - 1))
+            rsem = new_sem()
+            for p in some:
+                to = to_sp(p)
+                push(src.at[rows_of_peer(to[0])], dst.at[p * unit:(p + 1) * unit], all_sent, rsem, to)
+            coming.append((dst.at[some[0] * unit:(some[-1] + 1) * unit], rsem) if some else None)
+        left.append((src.at[0:(nsp - 1) * unit], all_sent))
+        dst[(nsp - 1) * unit:nsp * unit] = src[rows_of_peer(sp)]
+        return coming
+
+    coming = to_experts(dsend, darr)
+    rowed = over_tp(lambda to: settled_cols.at[rows_at(to)], settled.at[:, lanes_of(tp)], settled_cols.at[0:(ntp - 1) * own_rows])
+    settled[:, lanes_of(tp)] = settled_cols[rows_at(tp)]
     phase("weights")
-    drain()
     share = af[0:1] + af[1:2]
     scaled = jnp.where(named[0], af[0:1] / share, 0.0) + jnp.where(named[1], af[1:2] / share, 0.0)
     scaled = scaled.T
@@ -417,13 +423,31 @@
     pick_hi[...] = high
     pick_lo[...] = (scaled - high.astype(F32)).astype(BF16)
 
+    phase("stats")
+    await_bytes(*rowed)
+    whole = settled[...]
+    mean = jnp.mean(whole, axis=-1, keepdims=True)
+    spread = jnp.mean(jnp.square(whole - mean), axis=-1, keepdims=True)
+    rate = lax.rsqrt(spread + 1e-05)
+    settled[...] = (whole - mean) * rate * gains[0:1]
+    lane = iota((own_rows, LANES), 1)
+    offset = jnp.zeros((own_rows, LANES), F32)
+    for k in range(ntp):
+        shift = jnp.mean(whole[:, k * LANES:(k + 1) * LANES], axis=-1, keepdims=True) - mean
+        offset = jnp.where((lane % ntp == k) & (lane < 3 * ntp), shift, offset)
+    coarse = offset.astype(BF16).astype(F32)
+    offset = jnp.where((lane >= ntp) & (lane < 2 * ntp), offset - coarse, coarse)
+    for k in range(3):
+        top = rate.astype(BF16).astype(F32)
+        offset = jnp.where(lane == 3 * ntp + k, top, offset)
+        rate = rate - top
+    own_stats[...] = offset.astype(BF16)
+    told = over_tp(lambda to: own_stats, stats.at[rows_at(tp)], stats.at[0:(ntp - 1) * own_rows])
+    stats[rows_at(tp)] = own_stats[...]
     phase("dispatch_wait")
 
     def chunk(q):
         return slice(q * crow, (q + 1) * crow)
-
-    def slot(place, core):
-        return 2 * place + core
 
     ring_sent, hand_sent = new_sem(), new_sem()
     counts_of = [0, 0]
@@ -475,8 +499,23 @@
         for item in passed:
             grow_acc(*item)
         passed = fresh
+        if h == 0:
+            await_bytes(*told)
+            xsend[...] = mm(chosen[...], stats[...]).astype(BF16).reshape(nrow // 8, 8, LANES)
+            facts = to_experts(xsend, xarr)
+            apart = jnp.where(iota((ntp, width), 1) // LANES == iota((ntp, width), 0), gains[0:1], 0.0)
+            coarse = apart.astype(BF16)
+            fine = (apart - coarse.astype(F32)).astype(BF16)
+            slope = mm(coarse, wgu[...]) + mm(fine, wgu[...])
+            coarse = slope.astype(BF16)
+            fine = (slope - coarse.astype(F32)).astype(BF16)
+            tilt[0:ntp], tilt[ntp:2 * ntp], tilt[2 * ntp:3 * ntp] = coarse, coarse, fine
+            tilt[3 * ntp:LANES] = jnp.zeros((LANES - 3 * ntp, 4 * LANES), BF16)
     for item in passed:
         grow_acc(*item)
+    for item in facts:
+        if item:
+            await_bytes(*item)
 
     def last_piece(q):
         way = 1 if q % 2 == 0 else -1
@@ -507,7 +546,9 @@
     def finish_rows(item):
         grow_acc(*item)
         q = item[1]
-        a = acc[chunk(q)]
+        told_rows = xarr[q * crow // 8:(q + 1) * crow // 8].reshape(crow, LANES)
+        rate = told_rows[:, 3 * ntp:3 * ntp + 3].astype(F32)
+        a = (acc[chunk(q)] + mm(told_rows, tilt[...])) * jnp.sum(rate, axis=-1, keepdims=True)
         for k in range(2):
             gate, up = a[:, 2 * k * LANES:(2 * k + 1) * LANES], a[:, (2 * k + 1) * LANES:(2 * k + 2) * LANES]
             act[chunk(q), k * LANES:(k + 1) * LANES] = (jax.nn.silu(gate) * up).astype(BF16)
@@ -549,7 +590,7 @@
     back = rback[...].reshape(nrow, LANES)
     term[...] = (mm(pick_hi[...], back) + mm(pick_lo[...], back)).astype(BF16)
     phase("mix_over_tp")
-    moved = over_tp(lambda to: term.at[rows_at(to)], mix.at[:, lanes_of(tp)])
+    moved = over_tp(lambda to: term.at[rows_at(to)], mix.at[:, lanes_of(tp)], cols.at[0:(ntp - 1) * own_rows])
     mix[:, lanes_of(tp)] = term[rows_at(tp)]
     await_bytes(*moved)
     phase("last_norm")
@@ -579,22 +620,24 @@
     operands = (q1, k1, v1, g1, d1, q2, k2, v2, g2, d2, one[0], p1, p2, st, one[1], one[2], one[3], one[4], eg, eu, ed)
     scratch = [
         V((2, *q1.shape), BF16), V((4, *q2.shape), BF16), V((2, *q2.shape), BF16), V(d1.shape, F32), V(d2.shape, F32),
-        V((1, LANES), F32), V((2 * LANES, width), BF16), V((2 * LANES, width), BF16), V((own_rows, width), BF16),
+        V((1, LANES), F32), V((2 * LANES, width), BF16), V((2 * LANES, width), BF16), V((toks, LANES), BF16),
         V((2, width), F32), V((2, toks), jnp.int32), V((2, toks), F32),
         V((width, 4 * LANES), BF16), V((2 * LANES, width), BF16),
         V((nsp, mrow, LANES), BF16), V((nsp, mrow, LANES), BF16), V((nsp, mrow, LANES), F32),
         V((nsp, mrow, LANES), BF16), V((nsp, mrow, LANES), BF16),
         V((3, toks, LANES), BF16), V((3, toks, LANES), BF16), V((3, toks // BLK, LANES, LANES), F32),
-        V((2, toks, LANES), F32), V((2, ny, own_rows, 2 * LANES), BF16), V((ny, own_rows, 2 * LANES), BF16),
-        V((ny, own_rows, width), F32),
-        V((2 * CHUNKS, steps, own_rows, width // CHUNKS), BF16), V((2 * CHUNKS, steps, own_rows, width // CHUNKS), BF16),
-        V((own_rows, width), F32), V((own_rows, width), BF16), V((toks, LANES), BF16),
+        V((2, toks, LANES), F32), V((toks, 2 * LANES), BF16), V((toks, 2 * LANES), BF16),
+        V((ny, toks, LANES), F32),
+        V((2 * CHUNKS, 4, toks // CHUNKS, LANES), BF16), V((2 * CHUNKS, 4, toks // CHUNKS, LANES), BF16),
+        V((own_rows, width), F32), V((toks, LANES), F32), V((own_rows, LANES), BF16), V((toks, LANES), BF16),
+        V((nrow, toks), BF16), V((nrow // 8, 8, LANES), BF16), V((nrow // 8, 8, LANES), BF16), V((LANES, 4 * LANES), BF16),
+        V((toks, LANES), BF16),
         V((nrow // 8, 8, LANES), BF16), V((nrow // 8, 8, LANES), BF16), V((ntp, nrow, LANES), BF16),
         V((nrow, 4 * LANES), F32), V((nrow, 2 * LANES), BF16),
         V((2 * CHUNKS, steps, nrow // CHUNKS, LANES), BF16), V((2 * CHUNKS, steps, nrow // CHUNKS, LANES), BF16),
         V((nrow // 8, 8, LANES), BF16), V((nrow // 8, 8, LANES), BF16),
         V((toks, nrow), BF16), V((toks, nrow), BF16), V((toks, LANES), BF16), V((own_rows, width), BF16),
-        D((156,)),
+        D((163,)),
     ]
     return pl.pallas_call(
         functools.partial(kernel, (nsp, 4 if nsp % 4 == 0 else 1, ntp, toks, cap)),

time: 107 us -> 100 us (0.935)
  Pallas kernels: 105 us -> 98.5 us
    pallas_call x1, Pallas kernels: 105 us -> 98.5 us  [layer(): pl.pallas_call(functools.partial(kernel, (nsp, 4 if nsp % 4 == 0 else 1,...]
where the time goes in v4:
time: 100 us
  Pallas kernels  98.5 us (98%)
  local copies, waits for them, and re-layouts  1.47 us (1%)
    pallas_call x1, Pallas kernels, layer(): pl.pallas_call(functools.partial(kernel, (nsp, 4 if nsp % 4 == 0 else 1,...  98.5 us

profile of v4, /device:TPU:1, one launch (start us, length us, event | category | flops | bytes accessed | tf_op | source)
XLA Modules:
  0.0 100.0 jit_solution(16022193180002860513)
XLA Ops:
  0.0 98.5 %layer.1 = bf16[16,2048]{1,0:T(8,128)(2,1)} custom-call(bf16[64,256]{1,0:T(8,128)(2,1)} %bitcast.11, bf16[64,256]{1,0:T(8,128)(2,1)} %bitcast.12, bf16[256,128]{1,0:T(8,128)(2,1)} %v1h.1, bf16[256,128]{1,0:T(8,128)(2,1)} %g1h.1, f32[128,256]{1,0:T(8,128)} %bitcast.10, bf16[256,128]{1,0:T(8,128)(2,1)} %q2h.1, bf16[256,128]{1,0:T(8,128)(2,1)} %k2h.1, ...), custom_call_target="tpu_custom_call" | custom-call | tf_op jit(solution)/shard_map/layer/pallas_call | solution.py:642
  98.5 1.5 %copy.23 = bf16[16,2048]{1,0:T(8,128)(2,1)} copy(bf16[16,2048]{1,0:T(8,128)(2,1)} %layer.1) | data formatting | bytes 131072

commit v5 on v4

--- a/solution.py
+++ b/solution.py
@@ -109,16 +109,16 @@
         return sem
 
     phase("greet")
+    barrier = pltpu.get_barrier_semaphore()
+    for move in sp_moves[:-1]:
+        pl.semaphore_signal(barrier, inc=1, device_id=(sp_peer(move, 1), tp), device_id_type=MESH)
+    for move in tp_moves[:-1]:
+        pl.semaphore_signal(barrier, inc=1, device_id=(sp, tp_peer(move)), device_id_type=MESH)
     first = [
         (d1, load((d1h, d1))), (d2, load((d2h, d2))),
         (wide_in, load((k2h, wide_in.at[0]), (v1h, wide_in.at[1]), (v2h, wide_in.at[2]), (q2h, wide_in.at[3]))),
         (qk1, load((q1h, qk1.at[0]), (k1h, qk1.at[1]))),
     ]
-    barrier = pltpu.get_barrier_semaphore()
-    for move in sp_moves[:-1]:
-        pl.semaphore_signal(barrier, inc=1, device_id=(sp_peer(move, 1), tp), device_id_type=MESH)
-    for move in tp_moves[:-1]:
-        pl.semaphore_signal(barrier, inc=1, device_id=(sp, tp_peer(move)), device_id_type=MESH)
     own_stream = sth.at[:, pl.ds(pl.multiple_of(tp * LANES, LANES), LANES)]
     second = [
         (gates, load((g1h, gates.at[0]), (g2h, gates.at[1]))), (hg, load((hgh, hg))),
@@ -297,6 +297,28 @@
         rt[k:k + 1] * cap + jnp.sum(hits[k] * counts, axis=0, keepdims=True).astype(jnp.int32) for k in range(2)
     ]
 
+    slots = iota((nrow, toks), 0)
+    named = [slots == places[k] for k in range(2)]
+    chosen[...] = jnp.where(named[0] | named[1], 1.0, 0.0).astype(BF16)
+    share = af[0:1] + af[1:2]
+    scaled = jnp.where(named[0], af[0:1] / share, 0.0) + jnp.where(named[1], af[1:2] / share, 0.0)
+    scaled = scaled.T
+    high = scaled.astype(BF16)
+    pick_hi[...] = high
+    pick_lo[...] = (scaled - high.astype(F32)).astype(BF16)
+
+    await_bytes(*lent_wgu)
+    apart = jnp.where(iota((ntp, width), 1) // LANES == iota((ntp, width), 0), gains[0:1], 0.0)
+    coarse = apart.astype(BF16)
+    fine = (apart - coarse.astype(F32)).astype(BF16)
+    slope = mm(coarse, wgu[...]) + mm(fine, wgu[...])
+    coarse = slope.astype(BF16)
+    fine = (slope - coarse.astype(F32)).astype(BF16)
+    tilt[0:ntp], tilt[ntp:2 * ntp], tilt[2 * ntp:3 * ntp] = coarse, coarse, fine
+    tilt[3 * ntp:LANES] = jnp.zeros((LANES - 3 * ntp, 4 * LANES), BF16)
+    await_bytes(*lent_proj)
+    await_bytes(*lent_down)
+
     phase("wait_back")
     await_bytes(*coming)
     phase("readout")
@@ -304,6 +326,7 @@
     come = [mm(unpack[g], back) for g in range(3)]
     fwd_a, back_a = chained(0, rise, come[0])[0], chained(0, fall, come[0])[0]
     fwd_b, back_b = chained(1, rise, come[1])[0], chained(2, fall, come[2])[0]
+    shared = []
     for b in range(blocks):
         at = slice(b * BLK, (b + 1) * BLK)
         one = mixed[0, at] + mm_t(qin[0, at], jnp.where(low, fwd_a[b], back_a[b]).astype(BF16))
@@ -314,10 +337,11 @@
             done.append((normed * jax.nn.silu(gate[at].astype(F32))).astype(BF16))
         for k in range(2):
             heads[at, k * LANES:(k + 1) * LANES] = done[k]
+        if b % 2:
+            both = slice((b - 1) * BLK, (b + 1) * BLK)
+            shared.append((both, lend(heads_in.at[both], (heads.at[both], heads_in.at[both]))))
 
     phase("proj")
-    shared = lend(heads_in, (heads, heads_in))
-
     def lanes_of(k):
         return pl.ds(pl.multiple_of(k * LANES, LANES), LANES)
 
@@ -327,12 +351,11 @@
     def slot(place, core):
         return 2 * place + core
 
-    for d in range(ny):
-        part[d] = mm(heads[...], own_proj[:, lanes_of(slot(d, c))])
-    await_bytes(*lent_proj)
-    await_bytes(*shared)
-    for d in range(ny):
-        part[d] = part[d] + mm(heads_in[...], other_proj[:, lanes_of(slot(d, c))])
+    order = (3, ny - 3, 4, 1, ny - 1, 2, ny - 2, 0)
+    far = [chip(d) for d in order]
+    for both, item in shared:
+        for d in far:
+            part[d, both] = mm(heads[both], own_proj[:, lanes_of(slot(d, c))])
 
     phase("attn_ring")
     chains = [(way, q, (q % 2 == 0) != (way == 1)) for q in range(CHUNKS) for way in (1, -1)]
@@ -347,36 +370,39 @@
     def span(q):
         return slice(q * tall, (q + 1) * tall)
 
-    def toward(n, kind, total, hops):
+    def toward(n, kind, total, hops, sem):
         way = chains[n][0]
-        sem = new_sem()
         pbuf[n, kind] = total.astype(BF16)
         push(pbuf.at[n, kind], parr.at[n, kind], all_sent, sem, at_chip(chip(way * hops)))
         pieces[0] += 1
-        return parr.at[n, kind], sem
-
-    def added(total, item):
+
+    early = [new_sem() for n in chains]
+    final = [new_sem() for q in range(CHUNKS)]
+    for both, item in shared:
         await_bytes(*item)
-        return total + item[0][...].astype(F32)
-
-    third, fourth, near, merged = {}, {}, {}, {}
+        for d in far:
+            part[d, both] = part[d, both] + mm(heads_in[both], other_proj[:, lanes_of(slot(d, c))])
+        for n, (way, q, skip) in enumerate(chains):
+            if both.start <= span(q).start < both.stop:
+                toward(n, 0, part[chip(3 * way), span(q)], 1, early[n])
+                if not skip:
+                    toward(n, 1, part[chip(4 * way), span(q)], 2, early[n])
     for n, (way, q, skip) in enumerate(chains):
-        third[n] = toward(n, 0, part[chip(3 * way), span(q)], 1)
-        if not skip:
-            fourth[n] = toward(n, 1, part[chip(4 * way), span(q)], 2)
+        toward(n, 2, part[chip(way), span(q)], 1, final[q])
     for n, (way, q, skip) in enumerate(chains):
-        near[n] = toward(n, 2, part[chip(way), span(q)], 1)
-    for n, (way, q, skip) in enumerate(chains):
-        total = added(part[chip(2 * way), span(q)], third[n])
-        if not skip:
-            total = added(total, fourth[n])
-        merged[n] = toward(n, 3, total, 2)
+        kinds = 1 if skip else 2
+        await_bytes(parr.at[n, 0:kinds], early[n])
+        total = part[chip(2 * way), span(q)]
+        for kind in range(kinds):
+            total = total + parr[n, kind].astype(F32)
+        toward(n, 3, total, 2, final[q])
     own_gain = gains[0:1, lanes_of(tp)]
     for q in range(CHUNKS):
         total = part[y, span(q)]
-        for items in (near, merged):
+        await_bytes(parr.at[0], final[q])
+        for kind in (2, 3):
             for way in (1, -1):
-                total = added(total, items[chain_no[way, q]])
+                total = total + parr[chain_no[way, q], kind].astype(F32)
         summed = stream[span(q)].astype(F32) + total.astype(BF16).astype(F32)
         settled_cols[span(q)] = summed
         cols[span(q)] = ((summed - jnp.mean(summed, axis=-1, keepdims=True)) * own_gain).astype(BF16)
@@ -391,11 +417,7 @@
         left.append((size, ssem))
         return size, rsem
 
-    slots = iota((nrow, toks), 0)
-    named = [slots == places[k] for k in range(2)]
-    gather = jnp.where(named[0] | named[1], 1.0, 0.0).astype(BF16)
-    chosen[...] = gather
-    dsend[...] = mm(gather, cols[...]).astype(BF16).reshape(nrow // 8, 8, LANES)
+    dsend[...] = mm(chosen[...], cols[...]).astype(BF16).reshape(nrow // 8, 8, LANES)
     unit = cap // 8
     rows_of_peer = lambda k: pl.ds(k * unit, unit)
 
@@ -415,14 +437,7 @@
     coming = to_experts(dsend, darr)
     rowed = over_tp(lambda to: settled_cols.at[rows_at(to)], settled.at[:, lanes_of(tp)], settled_cols.at[0:(ntp - 1) * own_rows])
     settled[:, lanes_of(tp)] = settled_cols[rows_at(tp)]
-    phase("weights")
-    share = af[0:1] + af[1:2]
-    scaled = jnp.where(named[0], af[0:1] / share, 0.0) + jnp.where(named[1], af[1:2] / share, 0.0)
-    scaled = scaled.T
-    high = scaled.astype(BF16)
-    pick_hi[...] = high
-    pick_lo[...] = (scaled - high.astype(F32)).astype(BF16)
-
+    drain()
     phase("stats")
     await_bytes(*rowed)
     whole = settled[...]
@@ -452,109 +467,111 @@
     ring_sent, hand_sent = new_sem(), new_sem()
     counts_of = [0, 0]
 
-    def hand_on(q, place):
-        at = rows.at[slot(place, c), chunk(q)]
-        rsem = new_sem()
-        push(at, at, hand_sent, rsem, sib)
-        counts_of[1] += 1
-        return rows.at[slot(place, 1 - c), chunk(q)], rsem
-
-    def ring(n, h):
-        way, q, skip = chains[n]
-        at = rows.at[slot(chip(-way * h), c), chunk(q)]
-        rsem = new_sem()
-        push(at, at, ring_sent, rsem, at_chip(chip(way)))
-        counts_of[0] += 1
-        return rows.at[slot(chip(-way * (h + 1)), c), chunk(q)], rsem
-
-    def grow_acc(copy, q, place, fresh=False):
-        await_bytes(*copy)
-        both = jnp.concatenate([rows[slot(place, 0), chunk(q)], rows[slot(place, 1), chunk(q)]], axis=1)
-        more = mm(both, wgu[pl.ds(pl.multiple_of(place * 2 * LANES, 2 * LANES), 2 * LANES)])
+    def ways_at(q, h):
+        return [way for way in (1, -1) if h < half_way - chains[chain_no[way, q]][2]]
+
+    def some_rows(count):
+        return rows.at[0, 0:count * crow]
+
+    def hand_on(q, spots):
+        sem = new_sem()
+        for place in spots:
+            at = rows.at[slot(place, c), chunk(q)]
+            push(at, at, hand_sent, sem, sib)
+            counts_of[1] += 1
+        return (some_rows(len(spots)), sem), q, spots
+
+    def ring(q, h):
+        sem = new_sem()
+        for way in ways_at(q, h):
+            at = rows.at[slot(chip(-way * h), c), chunk(q)]
+            push(at, at, ring_sent, sem, at_chip(chip(way)))
+            counts_of[0] += 1
+        return some_rows(len(ways_at(q, h))), sem
+
+    def grow_acc(item, q, spots, fresh=False):
+        await_bytes(*item)
+        more = None
+        for place in spots:
+            both = jnp.concatenate([rows[slot(place, 0), chunk(q)], rows[slot(place, 1), chunk(q)]], axis=1)
+            one = mm(both, wgu[pl.ds(pl.multiple_of(place * 2 * LANES, 2 * LANES), 2 * LANES)])
+            more = one if more is None else more + one
         acc[chunk(q)] = more if fresh else acc[chunk(q)] + more
 
-    link, passed = {}, []
+    link, passed = [], []
     for q in range(CHUNKS):
         if coming[q]:
             await_bytes(*coming[q])
         rows[tp, chunk(q)] = darr[q * crow // 8:(q + 1) * crow // 8].reshape(crow, LANES)
-        for way in (1, -1):
-            n = chain_no[way, q]
-            if half_way - chains[n][2] > 0:
-                link[n] = ring(n, 0)
-        passed.append((hand_on(q, y), q, y, True))
+        link.append(ring(q, 0))
+        passed.append((*hand_on(q, [y]), True))
     phase("gather_ring")
-    await_bytes(*lent_wgu)
-    await_bytes(*lent_down)
     for h in range(half_way - 1):
         fresh = []
-        for n, (way, q, skip) in enumerate(chains):
-            if h >= half_way - skip:
-                continue
-            await_bytes(*link[n])
-            if h + 1 < half_way - skip:
-                link[n] = ring(n, h + 1)
-            place = chip(-way * (h + 1))
-            fresh.append((hand_on(q, place), q, place))
-        for item in passed:
-            grow_acc(*item)
+        for q in range(CHUNKS):
+            await_bytes(*link[q])
+            if ways_at(q, h + 1):
+                link[q] = ring(q, h + 1)
+            fresh.append(hand_on(q, [chip(-way * (h + 1)) for way in ways_at(q, h)]))
+            if h == 0 and q == 1:
+                await_bytes(*told)
+                xsend[...] = mm(chosen[...], stats[...]).astype(BF16).reshape(nrow // 8, 8, LANES)
+                facts = to_experts(xsend, xarr)
+            if h > 0:
+                grow_acc(*passed[q])
+        if h == 0:
+            for item in passed:
+                grow_acc(*item)
         passed = fresh
-        if h == 0:
-            await_bytes(*told)
-            xsend[...] = mm(chosen[...], stats[...]).astype(BF16).reshape(nrow // 8, 8, LANES)
-            facts = to_experts(xsend, xarr)
-            apart = jnp.where(iota((ntp, width), 1) // LANES == iota((ntp, width), 0), gains[0:1], 0.0)
-            coarse = apart.astype(BF16)
-            fine = (apart - coarse.astype(F32)).astype(BF16)
-            slope = mm(coarse, wgu[...]) + mm(fine, wgu[...])
-            coarse = slope.astype(BF16)
-            fine = (slope - coarse.astype(F32)).astype(BF16)
-            tilt[0:ntp], tilt[ntp:2 * ntp], tilt[2 * ntp:3 * ntp] = coarse, coarse, fine
-            tilt[3 * ntp:LANES] = jnp.zeros((LANES - 3 * ntp, 4 * LANES), BF16)
-    for item in passed:
-        grow_acc(*item)
-    for item in facts:
-        if item:
-            await_bytes(*item)
+    for q in range(CHUNKS):
+        grow_acc(*passed[q])
 
     def last_piece(q):
-        way = 1 if q % 2 == 0 else -1
-        n = chain_no[way, q]
-        await_bytes(*link[n])
-        place = chip(half_way)
-        return hand_on(q, place), q, place
+        await_bytes(*link[q])
+        return hand_on(q, [chip(half_way)])
 
     def own_part(place, q):
         return mm(act[chunk(q)], down[:, lanes_of(slot(place, c))])
 
     sent, reduced, all_sent = {}, [0], new_sem()
 
-    def reduce_step(n, t):
-        way, q, skip = chains[n]
-        h = t + skip
-        if h >= half_way:
-            return
-        total = own_part(chip(way * (half_way - h)), q)
+    def landed(q, t):
+        await_bytes(rarr.at[0, 0:len(ways_at(q, t))], sent[q])
+
+    def reduce_step(q, t):
+        ways = ways_at(q, t)
+        where = {way: t + chains[chain_no[way, q]][2] for way in ways}
+        totals = {way: own_part(chip(way * (half_way - where[way])), q) for way in ways}
         if t > 0:
-            await_bytes(rarr.at[n, h - 1], sent[n])
-            total = total + rarr[n, h - 1].astype(F32)
-        rbuf[n, h] = total.astype(BF16)
-        sent[n] = new_sem()
-        push(rbuf.at[n, h], rarr.at[n, h], all_sent, sent[n], at_chip(chip(way)))
-        reduced[0] += 1
+            landed(q, t - 1)
+        sent[q] = new_sem()
+        for way in ways:
+            n, h = chain_no[way, q], where[way]
+            total = totals[way]
+            if t > 0:
+                total = total + rarr[n, h - 1].astype(F32)
+            rbuf[n, h] = total.astype(BF16)
+            push(rbuf.at[n, h], rarr.at[n, h], all_sent, sent[q], at_chip(chip(way)))
+            reduced[0] += 1
+
+    def told_rows(q):
+        return xarr[q * crow // 8:(q + 1) * crow // 8].reshape(crow, LANES)
 
     def finish_rows(item):
         grow_acc(*item)
         q = item[1]
-        told_rows = xarr[q * crow // 8:(q + 1) * crow // 8].reshape(crow, LANES)
-        rate = told_rows[:, 3 * ntp:3 * ntp + 3].astype(F32)
-        a = (acc[chunk(q)] + mm(told_rows, tilt[...])) * jnp.sum(rate, axis=-1, keepdims=True)
+        rate = told_rows(q)[:, 3 * ntp:3 * ntp + 3].astype(F32)
+        a = acc[chunk(q)] * jnp.sum(rate, axis=-1, keepdims=True)
         for k in range(2):
             gate, up = a[:, 2 * k * LANES:(2 * k + 1) * LANES], a[:, (2 * k + 1) * LANES:(2 * k + 2) * LANES]
             act[chunk(q), k * LANES:(k + 1) * LANES] = (jax.nn.silu(gate) * up).astype(BF16)
-        for way in (1, -1):
-            reduce_step(chain_no[way, q], 0)
-
+        reduce_step(q, 0)
+
+    phase("facts")
+    for q in range(CHUNKS):
+        if facts[q]:
+            await_bytes(*facts[q])
+        acc[chunk(q)] = acc[chunk(q)] + mm(told_rows(q), tilt[...])
     drain()
     phase("last_pieces")
     waiting = [last_piece(0)]
@@ -564,19 +581,17 @@
     finish_rows(waiting[CHUNKS - 1])
     phase("reduce_ring")
     for t in range(1, half_way):
-        for n in range(len(chains)):
-            reduce_step(n, t)
+        for q in range(CHUNKS):
+            reduce_step(q, t)
     left.append((rbuf.at[0:reduced[0] // half_way], all_sent))
     left.append((rows.at[0:counts_of[0] // CHUNKS], ring_sent))
     left.append((rows.at[0:counts_of[1] // CHUNKS], hand_sent))
     all_sent, arrived = new_sem(), new_sem()
     for q in range(CHUNKS):
         total = own_part(y, q)
+        landed(q, half_way - 1)
         for way in (1, -1):
-            n = chain_no[way, q]
-            if n in sent:
-                await_bytes(rarr.at[n, half_way - 1], sent[n])
-                total = total + rarr[n, half_way - 1].astype(F32)
+            total = total + rarr[chain_no[way, q], half_way - 1].astype(F32)
         rsend[q * crow // 8:(q + 1) * crow // 8] = total.astype(BF16).reshape(crow // 8, 8, LANES)
         for p in range(q * nsp // CHUNKS, min((q + 1) * nsp // CHUNKS, nsp - 1)):
             push(rsend.at[p * unit:(p + 1) * unit], rback.at[rows_of_peer(sp)], all_sent, arrived, to_sp(p, -1))
@@ -637,7 +652,7 @@
         V((2 * CHUNKS, steps, nrow // CHUNKS, LANES), BF16), V((2 * CHUNKS, steps, nrow // CHUNKS, LANES), BF16),
         V((nrow // 8, 8, LANES), BF16), V((nrow // 8, 8, LANES), BF16),
         V((toks, nrow), BF16), V((toks, nrow), BF16), V((toks, LANES), BF16), V((own_rows, width), BF16),
-        D((163,)),
+        D((113,)),
     ]
     return pl.pallas_call(
         functools.partial(kernel, (nsp, 4 if nsp % 4 == 0 else 1, ntp, toks, cap)),

time: 100 us -> 98.5 us (0.985)
  Pallas kernels: 98.5 us -> 96.8 us
    pallas_call x1, Pallas kernels: 98.5 us -> 96.8 us  [layer(): pl.pallas_call(functools.partial(kernel, (nsp, 4 if nsp % 4 == 0 else 1,...]
where the time goes in v5:
time: 98.5 us; the launch traced here: 98.3 us
  Pallas kernels  96.8 us (98%)
  local copies, waits for them, and re-layouts  1.47 us (1%)
    pallas_call x1, Pallas kernels, layer(): pl.pallas_call(functools.partial(kernel, (nsp, 4 if nsp % 4 == 0 else 1,...  96.8 us

profile of v5, /device:TPU:1, one launch (start us, length us, event | category | flops | bytes accessed | tf_op | source)
XLA Modules:
  0.0 98.3 jit_solution(8815158440858997435)
XLA Ops:
  0.0 96.8 %layer.1 = bf16[16,2048]{1,0:T(8,128)(2,1)} custom-call(bf16[64,256]{1,0:T(8,128)(2,1)} %bitcast.11, bf16[64,256]{1,0:T(8,128)(2,1)} %bitcast.12, bf16[256,128]{1,0:T(8,128)(2,1)} %v1h.1, bf16[256,128]{1,0:T(8,128)(2,1)} %g1h.1, f32[128,256]{1,0:T(8,128)} %bitcast.10, bf16[256,128]{1,0:T(8,128)(2,1)} %q2h.1, bf16[256,128]{1,0:T(8,128)(2,1)} %k2h.1, ...), custom_call_target="tpu_custom_call" | custom-call | tf_op jit(solution)/shard_map/layer/pallas_call | solution.py:657
  96.9 1.5 %copy.23 = bf16[16,2048]{1,0:T(8,128)(2,1)} copy(bf16[16,2048]{1,0:T(8,128)(2,1)} %layer.1) | data formatting | bytes 131072

commit v6 on v5

--- a/solution.py
+++ b/solution.py
@@ -256,6 +256,26 @@
         score = jnp.where(lower, mm_t(qin[1, at], kin[1, at]), 0.0) + jnp.where(upper, mm_t(qin[2, at], kin[2, at]), 0.0)
         mixed[1, at] = mm(score.astype(BF16), values[1][at])
 
+    def reached(g, order):
+        share = jnp.ones((1, LANES), F32)
+        seen = {}
+        for b in order:
+            seen[b] = share
+            share = share * fades[g][b]
+        return seen
+
+    rise_a, fall_a = chained(0, rise, zero)[0], chained(0, fall, zero)[0]
+    rise_b, fall_b = chained(1, rise, zero)[0], chained(2, fall, zero)[0]
+    reach = [
+        {b: jnp.where(low, reached(0, rise)[b], reached(0, fall)[b]) for b in rise}, reached(1, rise), reached(2, fall)
+    ]
+    for b in range(blocks):
+        at = slice(b * BLK, (b + 1) * BLK)
+        mixed[0, at] = mixed[0, at] + mm_t(qin[0, at], jnp.where(low, rise_a[b], fall_a[b]).astype(BF16))
+        mixed[1, at] = mixed[1, at] + mm_t(qin[1, at], rise_b[b].astype(BF16)) + mm_t(qin[2, at], fall_b[b].astype(BF16))
+        for g in range(3):
+            qin[g, at] = (qin[g, at].astype(F32) * reach[g][b]).astype(BF16)
+
     phase("wait_states")
     await_bytes(*coming)
     phase("scan")
@@ -293,19 +313,22 @@
     hits = [jnp.where(rt[k:k + 1] == experts, 1.0, 0.0) for k in range(2)]
     before = jnp.where(r < s, 1.0, 0.0).astype(BF16)
     counts = mm((hits[0] + hits[1]).astype(BF16), before)
-    places = [
-        rt[k:k + 1] * cap + jnp.sum(hits[k] * counts, axis=0, keepdims=True).astype(jnp.int32) for k in range(2)
-    ]
+    spot = jnp.zeros((nsp, toks), jnp.int32)
+    for p, move in enumerate(sp_moves):
+        spot = jnp.where(experts == sp_peer(move, 1), p * cap, spot)
+    counts = counts + spot.astype(F32)
+    places = [jnp.sum(hits[k] * counts, axis=0, keepdims=True).astype(jnp.int32) for k in range(2)]
 
     slots = iota((nrow, toks), 0)
     named = [slots == places[k] for k in range(2)]
     chosen[...] = jnp.where(named[0] | named[1], 1.0, 0.0).astype(BF16)
     share = af[0:1] + af[1:2]
     scaled = jnp.where(named[0], af[0:1] / share, 0.0) + jnp.where(named[1], af[1:2] / share, 0.0)
-    scaled = scaled.T
-    high = scaled.astype(BF16)
-    pick_hi[...] = high
-    pick_lo[...] = (scaled - high.astype(F32)).astype(BF16)
+    for q in range(CHUNKS):
+        some = scaled[q * crow:(q + 1) * crow].T
+        high = some.astype(BF16)
+        pick_hi[q] = high
+        pick_lo[q] = (some - high.astype(F32)).astype(BF16)
 
     await_bytes(*lent_wgu)
     apart = jnp.where(iota((ntp, width), 1) // LANES == iota((ntp, width), 0), gains[0:1], 0.0)
@@ -323,23 +346,16 @@
     await_bytes(*coming)
     phase("readout")
     back = sback[...].reshape(nsp * mrow, LANES)
-    come = [mm(unpack[g], back) for g in range(3)]
-    fwd_a, back_a = chained(0, rise, come[0])[0], chained(0, fall, come[0])[0]
-    fwd_b, back_b = chained(1, rise, come[1])[0], chained(2, fall, come[2])[0]
+    come = [mm(unpack[g], back).astype(BF16) for g in range(3)]
     shared = []
-    for b in range(blocks):
-        at = slice(b * BLK, (b + 1) * BLK)
-        one = mixed[0, at] + mm_t(qin[0, at], jnp.where(low, fwd_a[b], back_a[b]).astype(BF16))
-        other = mixed[1, at] + mm_t(qin[1, at], fwd_b[b].astype(BF16)) + mm_t(qin[2, at], back_b[b].astype(BF16))
-        done = []
-        for value, gate in ((one, gates.at[0]), (other, gates.at[1])):
+    for n in range(2):
+        at = slice(n * toks // 2, (n + 1) * toks // 2)
+        one = mixed[0, at] + mm_t(qin[0, at], come[0])
+        other = mixed[1, at] + mm_t(qin[1, at], come[1]) + mm_t(qin[2, at], come[2])
+        for k, (value, gate) in enumerate(((one, gates.at[0]), (other, gates.at[1]))):
             normed = value * lax.rsqrt(jnp.mean(value * value, axis=-1, keepdims=True) + 1e-06) * hg[...]
-            done.append((normed * jax.nn.silu(gate[at].astype(F32))).astype(BF16))
-        for k in range(2):
-            heads[at, k * LANES:(k + 1) * LANES] = done[k]
-        if b % 2:
-            both = slice((b - 1) * BLK, (b + 1) * BLK)
-            shared.append((both, lend(heads_in.at[both], (heads.at[both], heads_in.at[both]))))
+            heads[at, k * LANES:(k + 1) * LANES] = (normed * jax.nn.silu(gate[at].astype(F32))).astype(BF16)
+        shared.append((at, lend(heads_in.at[at], (heads.at[at], heads_in.at[at]))))
 
     phase("proj")
     def lanes_of(k):
@@ -417,24 +433,31 @@
         left.append((size, ssem))
         return size, rsem
 
-    dsend[...] = mm(chosen[...], cols[...]).astype(BF16).reshape(nrow // 8, 8, LANES)
     unit = cap // 8
-    rows_of_peer = lambda k: pl.ds(k * unit, unit)
-
-    def to_experts(src, dst):
+
+    def chunk(q):
+        return slice(q * crow, (q + 1) * crow)
+
+    def units(q):
+        return slice(q * crow // 8, (q + 1) * crow // 8)
+
+    def peers(q):
+        return range(q * nsp // CHUNKS, min((q + 1) * nsp // CHUNKS, nsp - 1))
+
+    def to_experts(values, src, dst):
         all_sent, coming = new_sem(), []
         for q in range(CHUNKS):
-            some = range(q * nsp // CHUNKS, min((q + 1) * nsp // CHUNKS, nsp - 1))
+            src[units(q)] = mm(chosen[chunk(q)], values[...]).astype(BF16).reshape(crow // 8, 8, LANES)
             rsem = new_sem()
-            for p in some:
-                to = to_sp(p)
-                push(src.at[rows_of_peer(to[0])], dst.at[p * unit:(p + 1) * unit], all_sent, rsem, to)
-            coming.append((dst.at[some[0] * unit:(some[-1] + 1) * unit], rsem) if some else None)
+            for p in peers(q):
+                at = slice(p * unit, (p + 1) * unit)
+                push(src.at[at], dst.at[at], all_sent, rsem, to_sp(p))
+            coming.append((dst.at[peers(q)[0] * unit:(peers(q)[-1] + 1) * unit], rsem) if peers(q) else None)
         left.append((src.at[0:(nsp - 1) * unit], all_sent))
-        dst[(nsp - 1) * unit:nsp * unit] = src[rows_of_peer(sp)]
+        dst[(nsp - 1) * unit:nsp * unit] = src[(nsp - 1) * unit:nsp * unit]
         return coming
 
-    coming = to_experts(dsend, darr)
+    coming = to_experts(cols, dsend, darr)
     rowed = over_tp(lambda to: settled_cols.at[rows_at(to)], settled.at[:, lanes_of(tp)], settled_cols.at[0:(ntp - 1) * own_rows])
     settled[:, lanes_of(tp)] = settled_cols[rows_at(tp)]
     drain()
@@ -461,9 +484,6 @@
     stats[rows_at(tp)] = own_stats[...]
     phase("dispatch_wait")
 
-    def chunk(q):
-        return slice(q * crow, (q + 1) * crow)
-
     ring_sent, hand_sent = new_sem(), new_sem()
     counts_of = [0, 0]
 
@@ -502,7 +522,7 @@
     for q in range(CHUNKS):
         if coming[q]:
             await_bytes(*coming[q])
-        rows[tp, chunk(q)] = darr[q * crow // 8:(q + 1) * crow // 8].reshape(crow, LANES)
+        rows[tp, chunk(q)] = darr[units(q)].reshape(crow, LANES)
         link.append(ring(q, 0))
         passed.append((*hand_on(q, [y]), True))
     phase("gather_ring")
@@ -515,8 +535,7 @@
             fresh.append(hand_on(q, [chip(-way * (h + 1)) for way in ways_at(q, h)]))
             if h == 0 and q == 1:
                 await_bytes(*told)
-                xsend[...] = mm(chosen[...], stats[...]).astype(BF16).reshape(nrow // 8, 8, LANES)
-                facts = to_experts(xsend, xarr)
+                facts = to_experts(stats, xsend, xarr)
             if h > 0:
                 grow_acc(*passed[q])
         if h == 0:
@@ -555,7 +574,7 @@
             reduced[0] += 1
 
     def told_rows(q):
-        return xarr[q * crow // 8:(q + 1) * crow // 8].reshape(crow, LANES)
+        return xarr[units(q)].reshape(crow, LANES)
 
     def finish_rows(item):
         grow_acc(*item)
@@ -586,24 +605,29 @@
     left.append((rbuf.at[0:reduced[0] // half_way], all_sent))
     left.append((rows.at[0:counts_of[0] // CHUNKS], ring_sent))
     left.append((rows.at[0:counts_of[1] // CHUNKS], hand_sent))
-    all_sent, arrived = new_sem(), new_sem()
+    all_sent, arrived = new_sem(), [new_sem() for q in range(CHUNKS)]
     for q in range(CHUNKS):
         total = own_part(y, q)
         landed(q, half_way - 1)
         for way in (1, -1):
             total = total + rarr[chain_no[way, q], half_way - 1].astype(F32)
-        rsend[q * crow // 8:(q + 1) * crow // 8] = total.astype(BF16).reshape(crow // 8, 8, LANES)
-        for p in range(q * nsp // CHUNKS, min((q + 1) * nsp // CHUNKS, nsp - 1)):
-            push(rsend.at[p * unit:(p + 1) * unit], rback.at[rows_of_peer(sp)], all_sent, arrived, to_sp(p, -1))
+        rsend[units(q)] = total.astype(BF16).reshape(crow // 8, 8, LANES)
+        for p in peers(q):
+            at = slice(p * unit, (p + 1) * unit)
+            push(rsend.at[at], rback.at[at], all_sent, arrived[q], to_sp(p, -1))
     left.append((rsend.at[0:(nsp - 1) * unit], all_sent))
-    rback[rows_of_peer(sp)] = rsend[(nsp - 1) * unit:nsp * unit]
+    rback[(nsp - 1) * unit:nsp * unit] = rsend[(nsp - 1) * unit:nsp * unit]
     phase("return_wait")
     drain()
-    await_bytes(rback.at[0:(nsp - 1) * unit], arrived)
+    total = None
+    for q in range(CHUNKS):
+        if peers(q):
+            await_bytes(rback.at[peers(q)[0] * unit:(peers(q)[-1] + 1) * unit], arrived[q])
+        back = rback[units(q)].reshape(crow, LANES)
+        more = mm(pick_hi[q], back) + mm(pick_lo[q], back)
+        total = more if total is None else total + more
     phase("combine")
-
-    back = rback[...].reshape(nrow, LANES)
-    term[...] = (mm(pick_hi[...], back) + mm(pick_lo[...], back)).astype(BF16)
+    term[...] = total.astype(BF16)
     phase("mix_over_tp")
     moved = over_tp(lambda to: term.at[rows_at(to)], mix.at[:, lanes_of(tp)], cols.at[0:(ntp - 1) * own_rows])
     mix[:, lanes_of(tp)] = term[rows_at(tp)]
@@ -651,8 +675,9 @@
         V((nrow, 4 * LANES), F32), V((nrow, 2 * LANES), BF16),
         V((2 * CHUNKS, steps, nrow // CHUNKS, LANES), BF16), V((2 * CHUNKS, steps, nrow // CHUNKS, LANES), BF16),
         V((nrow // 8, 8, LANES), BF16), V((nrow // 8, 8, LANES), BF16),
-        V((toks, nrow), BF16), V((toks, nrow), BF16), V((toks, LANES), BF16), V((own_rows, width), BF16),
-        D((113,)),
+        V((CHUNKS, toks, nrow // CHUNKS), BF16), V((CHUNKS, toks, nrow // CHUNKS), BF16),
+        V((toks, LANES), BF16), V((own_rows, width), BF16),
+        D((116,)),
     ]
     return pl.pallas_call(
         functools.partial(kernel, (nsp, 4 if nsp % 4 == 0 else 1, ntp, toks, cap)),
@@ -660,9 +685,9 @@
         in_specs=[pl.BlockSpec(memory_space=ANY)] * len(operands),
         out_specs=pl.BlockSpec(memory_space=pltpu.VMEM),
         scratch_shapes=scratch,
-        compiler_params=pltpu.CompilerParams(collective_id=0, has_side_effects=True, vmem_limit_bytes=60 * 1024 * 1024),
+        compiler_params=pltpu.CompilerParams(collective_id=0, has_side_effects=True, vmem_limit_bytes=48 * 1024 * 1024),
         name="layer",
-    )(*operands)
+    )(*[pltpu.with_memory_space_constraint(a, pltpu.HBM) for a in operands])
 
 
 def solution(mesh):

time: 98.5 us -> 97.5 us (0.990)
  no operation moved by 1% of the time
where the time goes in v6:
time: 97.5 us; the launch traced here: 97.4 us
  Pallas kernels  96.7 us (99%)
    pallas_call x1, Pallas kernels, layer(): pl.pallas_call(functools.partial(kernel, (nsp, 4 if nsp % 4 == 0 else 1,...  96.7 us

profile of v6, /device:TPU:1, one launch (start us, length us, event | category | flops | bytes accessed | tf_op | source)
XLA Modules:
  0.0 97.4 jit_solution(14889536988670717859)
XLA Ops:
  0.0 96.7 %layer.1 = bf16[16,2048]{1,0:T(8,128)(2,1)S(1)} custom-call(bf16[64,256]{1,0:T(8,128)(2,1)} %bitcast.11, bf16[64,256]{1,0:T(8,128)(2,1)} %bitcast.12, bf16[256,128]{1,0:T(8,128)(2,1)} %v1h.1, bf16[256,128]{1,0:T(8,128)(2,1)} %g1h.1, f32[128,256]{1,0:T(8,128)} %bitcast.10, bf16[256,128]{1,0:T(8,128)(2,1)} %q2h.1, bf16[256,128]{1,0:T(8,128)(2,1)} %k2h.1, ...), custom_call_target="tpu_custom_call" | custom-call | tf_op jit(solution)/shard_map/layer/pallas_call | solution.py:682
  96.8 0.6 copy.23

commit v7 on v6

--- a/solution.py
+++ b/solution.py
@@ -542,9 +542,6 @@
             for item in passed:
                 grow_acc(*item)
         passed = fresh
-    for q in range(CHUNKS):
-        grow_acc(*passed[q])
-
     def last_piece(q):
         await_bytes(*link[q])
         return hand_on(q, [chip(half_way)])
@@ -592,6 +589,8 @@
             await_bytes(*facts[q])
         acc[chunk(q)] = acc[chunk(q)] + mm(told_rows(q), tilt[...])
     drain()
+    for q in range(CHUNKS):
+        grow_acc(*passed[q])
     phase("last_pieces")
     waiting = [last_piece(0)]
     for q in range(1, CHUNKS):

time: 97.5 us -> 97.1 us (level)
  no operation moved by 1% of the time
where the time goes in v7:
time: 97.1 us; the launch traced here: 97 us
  Pallas kernels  96.4 us (99%)
    pallas_call x1, Pallas kernels, layer(): pl.pallas_call(functools.partial(kernel, (nsp, 4 if nsp % 4 == 0 else 1,...  96.4 us

profile of v7, /device:TPU:1, one launch (start us, length us, event | category | flops | bytes accessed | tf_op | source)
XLA Modules:
  0.0 97.0 jit_solution(51243049511915431)
XLA Ops:
  0.0 96.4 %layer.1 = bf16[16,2048]{1,0:T(8,128)(2,1)S(1)} custom-call(bf16[64,256]{1,0:T(8,128)(2,1)} %bitcast.11, bf16[64,256]{1,0:T(8,128)(2,1)} %bitcast.12, bf16[256,128]{1,0:T(8,128)(2,1)} %v1h.1, bf16[256,128]{1,0:T(8,128)(2,1)} %g1h.1, f32[128,256]{1,0:T(8,128)} %bitcast.10, bf16[256,128]{1,0:T(8,128)(2,1)} %q2h.1, bf16[256,128]{1,0:T(8,128)(2,1)} %k2h.1, ...), custom_call_target="tpu_custom_call" | custom-call | tf_op jit(solution)/shard_map/layer/pallas_call | solution.py:681
  96.4 0.6 copy.23
